TPU v7x, 256 devices: a whole 4x4x8 slice. The times are simulated.
256 devices in a mesh: ep: 64 (over z, y, core), tp: 4 (over x).
Axes of the slice: x: 4, y: 4, z: 8, core: 2. Of those that a mesh axis runs over, the one named last changes fastest.
Arguments:
- tokens: bfloat16 [1024, 2048], P('ep'), may hold values from -6 to 6
- recur_state: float32 [1024, 8, 128, 128], P('ep', 'tp'), may hold values from -0.4 to 0.4
- attn_gain: float32 [2048], replicated, may hold values from 0.1 to 1.9
- query_weight: bfloat16 [2048, 1024], P(None, 'tp'), may hold values from -0.125 to 0.125
- key_weight: bfloat16 [2048, 1024], P(None, 'tp'), may hold values from -0.125 to 0.125
- value_weight: bfloat16 [2048, 1024], P(None, 'tp'), may hold values from -0.125 to 0.125
- outgate_weight: bfloat16 [2048, 1024], P(None, 'tp'), may hold values from -0.125 to 0.125
- beta_weight: bfloat16 [2048, 8], replicated, may hold values from -0.125 to 0.125
- decay_weight: bfloat16 [2048, 8], replicated, may hold values from -0.125 to 0.125
- decay_rate: float32 [8], replicated, may hold values from 0.05 to 2
- head_gain: float32 [128], replicated, may hold values from 0.1 to 1.9
- output_weight: bfloat16 [1024, 2048], P('tp'), may hold values from -0.1875 to 0.1875
- ffn_gain: float32 [2048], replicated, may hold values from 0.1 to 1.9
- routes: int32 [1024, 2], P('ep'), may hold values from 0 to 15, all different within a row; in each aligned block of 16 rows (0 to 15, 16 to 31, ...) at most 4 rows name the same one
- route_weight: float32 [1024, 2], P('ep'), may hold values from 0.2 to 1
- expert_gate: bfloat16 [64, 2048, 1024], P('ep', None, 'tp'), may hold values from -0.125 to 0.125
- expert_up: bfloat16 [64, 2048, 1024], P('ep', None, 'tp'), may hold values from -0.125 to 0.125
- expert_down: bfloat16 [64, 1024, 2048], P('ep', 'tp'), may hold values from -0.09375 to 0.09375
Outputs:
- mixed: bfloat16 [1024, 2048], P('ep', 'tp')
- new_state: float32 [1024, 8, 128, 128], P('ep', 'tp')
Inputs may be any that keep to these rules, and one draw needn't show every extreme that they name: `routes`: each row names 2 different experts; in each aligned block of 16 rows no expert is named by more than 4 rows.
All inputs are finite; a program needn't handle non-finite values.
Results may differ from a plain program's by a relative error of at most 0.014.
Values may be sent and summed in bfloat16 or wider, within the bound.
A program may use at most 64 MiB of HBM per device.

v0:
```python
import jax
import jax.numpy as jnp
from jax import lax
from jax.sharding import PartitionSpec as P

EPS = 1e-06


def copy_for_each(value, axis):
    length = lax.axis_size(axis)
    return lax.all_to_all(
        jnp.broadcast_to(value[None], (length, *value.shape)), axis, 0, 0, tiled=True
    )


def of_everyone(value, axis):
    everything = copy_for_each(value, axis)
    return jnp.sum(everything, axis=0)


def split_up(value, dim, length):
    before, after = (value.shape[:dim], value.shape[dim + 1 :])
    return jnp.moveaxis(value.reshape(*before, length, -1, *after), dim, 0)


def sent_and_summed(value, axis, dim):
    blocks = split_up(value, dim, lax.axis_size(axis))
    arrived = lax.all_to_all(blocks, axis, split_axis=0, concat_axis=0, tiled=True)
    return arrived.astype(jnp.float32).sum(axis=0)


def rms_scale(values, gain):
    return values * lax.rsqrt(jnp.mean(values * values, axis=-1, keepdims=True) + EPS) * gain


def unit_rows(values):
    return values * lax.rsqrt(jnp.sum(values * values, axis=-1, keepdims=True) + EPS)


def slot_targets(group_routes, experts, capacity):
    flat = group_routes.reshape(-1)
    onehot = (flat[:, None] == jnp.arange(experts, dtype=jnp.int32)[None, :]).astype(jnp.int32)
    running = jnp.cumsum(onehot, axis=0)
    position = jnp.sum(running * onehot, axis=1) - 1
    return (flat * capacity + position).reshape(group_routes.shape)


def local(
    tokens,
    recur_state,
    attn_gain,
    query_weight,
    key_weight,
    value_weight,
    outgate_weight,
    beta_weight,
    decay_weight,
    decay_rate,
    head_gain,
    output_weight,
    ffn_gain,
    routes,
    route_weight,
    expert_gate,
    expert_up,
    expert_down,
):
    f32 = jnp.float32
    bf16 = jnp.bfloat16
    highest = lax.Precision.HIGHEST
    seq_count, model_width = tokens.shape
    heads_here = recur_state.shape[1]
    head_size = recur_state.shape[2]
    groups = lax.axis_size("ep")
    lanes = lax.axis_size("tp")
    lane_index = lax.axis_index("tp")
    normed = rms_scale(tokens.astype(f32), attn_gain).astype(bf16)
    qproj = jnp.dot(normed, query_weight, preferred_element_type=f32).astype(bf16)
    kproj = jnp.dot(normed, key_weight, preferred_element_type=f32).astype(bf16)
    vproj = jnp.dot(normed, value_weight, preferred_element_type=f32).astype(bf16)
    zproj = jnp.dot(normed, outgate_weight, preferred_element_type=f32).astype(bf16)
    first_head = lane_index * heads_here
    own_beta = lax.dynamic_slice_in_dim(beta_weight, first_head, heads_here, 1)
    own_decay = lax.dynamic_slice_in_dim(decay_weight, first_head, heads_here, 1)
    own_rate = lax.dynamic_slice_in_dim(decay_rate, first_head, heads_here, 0)
    strength = jax.nn.sigmoid(jnp.dot(normed, own_beta, preferred_element_type=f32))
    fading = jnp.exp(
        -own_rate * jax.nn.softplus(jnp.dot(normed, own_decay, preferred_element_type=f32))
    )

    def split_heads(proj):
        return proj.astype(f32).reshape(seq_count, heads_here, head_size)

    query = unit_rows(jax.nn.silu(split_heads(qproj))) * head_size ** (-0.5)
    keyvec = unit_rows(jax.nn.silu(split_heads(kproj)))
    value = jax.nn.silu(split_heads(vproj))
    recall = jnp.einsum("thd,thde->the", keyvec, recur_state, precision=highest)
    written = (strength[..., None] * keyvec)[..., :, None] * (value - fading[..., None] * recall)[
        ..., None, :
    ]
    new_state = fading[..., None, None] * recur_state + written
    readout = jnp.einsum("thd,thde->the", query, new_state, precision=highest)
    headed = (
        (rms_scale(readout, head_gain) * jax.nn.silu(split_heads(zproj)))
        .reshape(seq_count, heads_here * head_size)
        .astype(bf16)
    )
    partial_out = jnp.dot(headed, output_weight, preferred_element_type=f32)
    branch = of_everyone(partial_out, "tp").astype(bf16)
    resid = (tokens.astype(f32) + branch.astype(f32)).astype(bf16)
    ffn_in = rms_scale(resid.astype(f32), ffn_gain).astype(bf16)
    top_count = routes.shape[1]
    experts = groups // 4
    capacity = min(seq_count, max(2, (2 * seq_count * top_count + experts - 1) // experts))
    quarter = model_width // lanes
    targets = slot_targets(routes, experts, capacity)
    slot_ids = jnp.arange(experts * capacity, dtype=jnp.int32)
    select = jnp.any(slot_ids[:, None, None] == targets[None, :, :], axis=-1).astype(bf16)
    gate_local = expert_gate[0]
    up_local = expert_up[0]
    down_local = expert_down[0]
    packed = jnp.dot(select, ffn_in, preferred_element_type=f32).astype(bf16)
    packed = packed.reshape(experts, 1, capacity, ffn_in.shape[1])
    packed = jnp.broadcast_to(packed, (experts, 4, capacity, ffn_in.shape[1]))
    arrived = lax.all_to_all(
        packed.reshape(groups, capacity, ffn_in.shape[1]),
        "ep",
        split_axis=0,
        concat_axis=0,
        tiled=True,
    ).reshape(groups * capacity, model_width)
    gated = jnp.dot(arrived, gate_local, preferred_element_type=f32)
    lifted = jnp.dot(arrived, up_local, preferred_element_type=f32)
    hidden = (jax.nn.silu(gated) * lifted).astype(bf16)
    slice_terms = jnp.dot(hidden, down_local, preferred_element_type=f32).reshape(
        groups, capacity, model_width
    )
    shares = sent_and_summed(slice_terms.astype(jnp.bfloat16), "tp", 2).astype(bf16)
    returned = lax.all_to_all(shares, "ep", split_axis=0, concat_axis=0, tiled=True)
    merged = (
        returned.astype(f32)
        .reshape(experts, 4, capacity, quarter)
        .sum(axis=1)
        .reshape(experts * capacity, quarter)
    )
    combine = jnp.zeros((seq_count, experts * capacity), f32)
    for choice_idx in range(top_count):
        match = (targets[:, choice_idx, None] == slot_ids[None, :]).astype(f32)
        combine = combine + route_weight[:, choice_idx, None] * match
    moe = jnp.dot(combine, merged, precision=highest)
    resid_own = lax.dynamic_slice_in_dim(resid, lane_index * quarter, quarter, 1)
    mixed = (resid_own.astype(f32) + moe).astype(bf16)
    return (mixed, new_state)


def solution(mesh):
    return jax.shard_map(
        local,
        mesh=mesh,
        in_specs=(
            P("ep", None),
            P("ep", "tp", None, None),
            P(),
            P(None, "tp"),
            P(None, "tp"),
            P(None, "tp"),
            P(None, "tp"),
            P(),
            P(),
            P(),
            P(),
            P("tp", None),
            P(),
            P("ep", None),
            P("ep", None),
            P("ep", None, "tp"),
            P("ep", None, "tp"),
            P("ep", "tp", None),
        ),
        out_specs=(P("ep", "tp"), P("ep", "tp", None, None)),
        check_vma=False,
    )
```

profile of v0, /device:TPU:1, one launch (start us, length us, event | category | flops | bytes accessed | tf_op | source)
XLA Modules:
  0.0 115.7 jit_solution(3458215373677482743)
XLA Ops:
  0.7 1.1 fusion.16
  1.8 1.1 fusion.8
  3.0 1.6 %fusion.4 = f32[16,256]{1,0:T(8,128)S(1)} fusion(bf16[2048,256]{1,0:T(8,128)(2,1)} %param.22, bf16[16,2048]{1,0:T(8,128)(2,1)} %param.18, f32[2048]{0:T(1024)} %param.20, f32[16]{0:T(128)S(1)} %add_rsqrt_fusion.4), kind=kOutput, calls=%fused_computation.12 | convolution fusion | flops 16916480 | bytes 1138752 | tf_op jit(solution)/shard_map/dot_general | solution.py:79
  4.7 0.7 dynamic-slice_negate_fusion
  5.4 1.1 fusion.44
  6.6 1.6 %fusion.3 = f32[16,256]{1,0:T(8,128)S(1)} fusion(bf16[2048,256]{1,0:T(8,128)(2,1)} %param.23, bf16[16,2048]{1,0:T(8,128)(2,1)} %param.18, f32[2048]{0:T(1024)} %param.20, f32[16]{0:T(128)S(1)} %add_rsqrt_fusion.4), kind=kOutput, calls=%fused_computation.10 | convolution fusion | flops 16916480 | bytes 1138752 | tf_op jit(solution)/shard_map/dot_general | solution.py:80
  8.2 1.5 %fusion.5 = f32[16,256]{1,0:T(8,128)S(1)} fusion(bf16[2048,256]{1,0:T(8,128)(2,1)} %param.21, bf16[16,2048]{1,0:T(8,128)(2,1)S(1)} %copy-done.3, f32[2048]{0:T(1024)S(1)} %copy-done.6, f32[16]{0:T(128)S(1)} %add_rsqrt_fusion.4), kind=kOutput, calls=%fused_computation.14 | convolution fusion | flops 16916480 | bytes 1138752 | tf_op jit(solution)/shard_map/dot_general | solution.py:78
  10.0 1.9 %fusion.57 = f32[16,2,1,128]{3,2,1,0:T(1,128)S(1)} fusion(f32[16,2,128,1]{2,3,1,0:T(1,128)S(1)} %bitcast.63, f32[16,2,128,128]{3,2,1,0:T(8,128)S(1)} %copy-done.1), kind=kOutput, calls=%fused_computation.92 | convolution fusion | flops 6291456 | bytes 2129920 | tf_op jit(solution)/shard_map/thd,thde->the/dot_general | solution.py:97
  11.9 0.7 multiply_add_fusion
  12.8 1.2 %copy-done.2 = f32[16,2,128,128]{3,2,1,0:T(8,128)} copy-done((f32[16,2,128,128]{3,2,1,0:T(8,128)}, f32[16,2,128,128]{3,2,1,0:T(8,128)S(1)}, u32[]{:S(2)}) %copy-start.2) | copy-done | bytes 2097176
  14.0 1.9 %fusion.58 = f32[16,2,1,128]{3,2,1,0:T(1,128)S(1)} fusion(f32[16,2,128,1]{2,3,1,0:T(1,128)S(1)} %bitcast.62, f32[16,2,128,128]{3,2,1,0:T(8,128)S(1)} %multiply_add_fusion), kind=kOutput, calls=%fused_computation.93 | convolution fusion | flops 6291456 | bytes 2129920 | tf_op jit(solution)/shard_map/thd,thde->the/dot_general | solution.py:102
  16.7 0.8 broadcast_in_dim.6
  17.5 4.8 %all-to-all-start = ((f32[4,16,2048]{2,1,0:T(8,128)}), f32[4,16,2048]{2,1,0:T(8,128)S(1)}, u32[]{:S(2)}, u32[]{:S(2)}) async-start(f32[4,16,2048]{2,1,0:T(8,128)} %broadcast_in_dim.6), calls=%async_computation | async-start | bytes 1048576 | tf_op jit(solution)/shard_map/all_to_all | solution.py:11
  23.1 6.7 %all-to-all-done = f32[4,16,2048]{2,1,0:T(8,128)S(1)} async-done(((f32[4,16,2048]{2,1,0:T(8,128)}), f32[4,16,2048]{2,1,0:T(8,128)S(1)}, u32[]{:S(2)}, u32[]{:S(2)}) %all-to-all-start) | async-done | bytes 524320 | tf_op jit(solution)/shard_map/all_to_all | solution.py:11
  30.4 0.5 broadcast_in_dim.8
  30.9 42.6 %all_to_all.20 = bf16[64,4,2048]{2,1,0:T(4,128)(2,1)S(1)} all-to-all(bf16[64,4,2048]{2,1,0:T(4,128)(2,1)S(1)} %bitcast.56), channel_id=1, replica_groups=mesh['ep'=64,'tp'=4] {'ep'}, dimensions={0} | all-to-all | bytes 2097152 | tf_op jit(solution)/shard_map/all_to_all | solution.py:125
  73.7 1.7 %fusion.11 = f32[256,256]{1,0:T(8,128)S(1)} fusion(bf16[256,2048]{1,0:T(8,128)(2,1)S(1)} %reshape.133, bf16[1,2048,256]{2,1,0:T(8,128)(2,1)} %param.33), kind=kOutput, calls=%fused_computation.22 | convolution fusion | flops 268435456 | bytes 2359296 | tf_op jit(solution)/shard_map/dot_general | solution.py:132
  75.5 0.4 fusion
  76.0 0.4 convolution_convert_fusion
  76.6 16.5 %all_to_all.21 = bf16[4,64,4,512]{3,1,2,0:T(8,128)(2,1)S(1)} all-to-all(bf16[4,64,4,512]{3,1,2,0:T(8,128)(2,1)S(1)} %bitcast.58), channel_id=1, replica_groups=mesh['ep'=64,'tp'=4] {'tp'}, dimensions={0} | all-to-all | bytes 2097152 | tf_op jit(solution)/shard_map/all_to_all | solution.py:28
  93.3 0.9 copy.87
  94.2 7.4 %all-to-all-start.3 = ((bf16[64,4,512]{2,1,0:T(4,128)(2,1)}), bf16[64,4,512]{2,1,0:T(4,128)(2,1)S(1)}, u32[]{:S(2)}, u32[]{:S(2)}) async-start(bf16[64,4,512]{2,1,0:T(4,128)(2,1)} %copy.87), calls=%async_computation.3 | async-start | bytes 524288 | tf_op jit(solution)/shard_map/all_to_all | solution.py:139
  101.6 13.0 %all-to-all-done.3 = bf16[64,4,512]{2,1,0:T(4,128)(2,1)S(1)} async-done(((bf16[64,4,512]{2,1,0:T(4,128)(2,1)}), bf16[64,4,512]{2,1,0:T(4,128)(2,1)S(1)}, u32[]{:S(2)}, u32[]{:S(2)}) %all-to-all-start.3) | async-done | bytes 262176 | tf_op jit(solution)/shard_map/all_to_all | solution.py:139
  114.8 0.9 fusion.1
  (65 shorter events, 3.6 us)
Async XLA Ops:
  0.6 75.4 %copy-start = (bf16[1,256,2048]{2,1,0:T(8,128)(2,1)S(1)}, bf16[1,256,2048]{2,1,0:T(8,128)(2,1)}, u32[]{:S(2)}) copy-start(bf16[1,256,2048]{2,1,0:T(8,128)(2,1)} %param.35) | copy-start | bytes 3145732
  0.6 7.5 %copy-start.3 = (bf16[16,2048]{1,0:T(8,128)(2,1)S(1)}, bf16[16,2048]{1,0:T(8,128)(2,1)}, u32[]{:S(2)}) copy-start(bf16[16,2048]{1,0:T(8,128)(2,1)} %param.18) | copy-start | bytes 196612
  0.7 7.5 %copy-start.6 = (f32[2048]{0:T(1024)S(1)}, f32[2048]{0:T(1024)}, u32[]{:S(2)}) copy-start(f32[2048]{0:T(1024)} %param.20) | copy-start | bytes 24580
  0.7 9.3 %copy-start.1 = (f32[16,2,128,128]{3,2,1,0:T(8,128)S(1)}, f32[16,2,128,128]{3,2,1,0:T(8,128)}, u32[]{:S(2)}) copy-start(f32[16,2,128,128]{3,2,1,0:T(8,128)} %param.19) | copy-start | bytes 6291460
  12.7 1.3 %copy-start.2 = (f32[16,2,128,128]{3,2,1,0:T(8,128)}, f32[16,2,128,128]{3,2,1,0:T(8,128)S(1)}, u32[]{:S(2)}) copy-start(f32[16,2,128,128]{3,2,1,0:T(8,128)S(1)} %multiply_add_fusion) | copy-start | bytes 6291460
  12.7 3.3 %copy-start.5 = (bf16[2048,256]{1,0:T(8,128)(2,1)S(1)}, bf16[2048,256]{1,0:T(8,128)(2,1)}, u32[]{:S(2)}) copy-start(bf16[2048,256]{1,0:T(8,128)(2,1)} %param.24) | copy-start | bytes 3145732
  12.7 3.6 %copy-start.10 = (f32[128]{0:T(128)S(1)}, f32[128]{0:T(128)}, u32[]{:S(2)}) copy-start(f32[128]{0:T(128)} %param.28) | copy-start | bytes 1540
  12.7 3.7 %copy-start.4 = (bf16[256,2048]{1,0:T(8,128)(2,1)S(1)}, bf16[256,2048]{1,0:T(8,128)(2,1)}, u32[]{:S(2)}) copy-start(bf16[256,2048]{1,0:T(8,128)(2,1)} %param.29) | copy-start | bytes 3145732
  15.9 6.5 %copy-start.8 = (s32[16,2]{0,1:T(2,128)S(1)}, s32[16,2]{0,1:T(2,128)}, u32[]{:S(2)}) copy-start(s32[16,2]{0,1:T(2,128)} %param.31) | copy-start | bytes 388
  16.3 13.7 %copy-start.7 = (f32[2048]{0:T(1024)S(1)}, f32[2048]{0:T(1024)}, u32[]{:S(2)}) copy-start(f32[2048]{0:T(1024)} %param.30) | copy-start | bytes 24580
  17.5 12.3 %all-to-all-start = ((f32[4,16,2048]{2,1,0:T(8,128)}), f32[4,16,2048]{2,1,0:T(8,128)S(1)}, u32[]{:S(2)}, u32[]{:S(2)}) async-start(f32[4,16,2048]{2,1,0:T(8,128)} %broadcast_in_dim.6), calls=%async_computation | async-start | bytes 1048576 | tf_op jit(solution)/shard_map/all_to_all | solution.py:11
  73.7 1.8 %copy-start.11 = (bf16[1,2048,256]{2,1,0:T(8,128)(2,1)S(1)}, bf16[1,2048,256]{2,1,0:T(8,128)(2,1)}, u32[]{:S(2)}) copy-start(bf16[1,2048,256]{2,1,0:T(8,128)(2,1)} %param.34) | copy-start | bytes 3145732
  76.6 25.0 %copy-start.9 = (f32[16,2]{0,1:T(2,128)S(1)}, f32[16,2]{0,1:T(2,128)}, u32[]{:S(2)}) copy-start(f32[16,2]{0,1:T(2,128)} %param.32) | copy-start | bytes 388
  94.2 20.5 %all-to-all-start.3 = ((bf16[64,4,512]{2,1,0:T(4,128)(2,1)}), bf16[64,4,512]{2,1,0:T(4,128)(2,1)S(1)}, u32[]{:S(2)}, u32[]{:S(2)}) async-start(bf16[64,4,512]{2,1,0:T(4,128)(2,1)} %copy.87), calls=%async_computation.3 | async-start | bytes 524288 | tf_op jit(solution)/shard_map/all_to_all | solution.py:139
where the time goes:
time: 116 us
  blocking collectives  59 us (51%)
  waiting for transfers between devices  19.8 us (17%)
  matrix products  14.8 us (13%)
  starting transfers between devices  12.2 us (11%)
  local copies, waits for them, and re-layouts  4.61 us (4%)
  other arithmetic  4.2 us (4%)
    all_to_all x1, blocking collectives, local(): lax.all_to_all(packed.reshape(groups, capacity, ffn_in.shape[1]), 'ep', s...  42.6 us
    all_to_all x1, blocking collectives, sent_and_summed(): lax.all_to_all(blocks, axis, split_axis=0, concat_axis=0, tiled=True)  16.5 us
    all_to_all x1, waiting for transfers between devices, local(): lax.all_to_all(shares, 'ep', split_axis=0, concat_axis=0, tiled=True)  13 us
    all_to_all x1, starting transfers between devices, local(): lax.all_to_all(shares, 'ep', split_axis=0, concat_axis=0, tiled=True)  7.38 us
    all_to_all x1, waiting for transfers between devices, copy_for_each(): lax.all_to_all(jnp.broadcast_to(value[None], (length, *value.shape)), axi...  6.72 us
    all_to_all x1, starting transfers between devices, copy_for_each(): lax.all_to_all(jnp.broadcast_to(value[None], (length, *value.shape)), axi...  4.83 us
  transfers between devices with their start and end apart: 2, of which 2 were waited for; matrix products, arithmetic and copies ran while one was open for 1% of the time, Pallas kernels for 0%

commit v1 on v0

v1 whole, which is shorter than its diff:
```python
import functools

import jax
import jax.numpy as jnp
from jax import lax
from jax.experimental import pallas as pl
from jax.experimental.pallas import tpu as pltpu
from jax.sharding import PartitionSpec as P

EPS = 1e-06
MESH = pl.DeviceIdType.MESH
F32 = jnp.float32
BF16 = jnp.bfloat16
CORES = 2
RING_Y = 4
CAP = 4
PARTS = 4
LANE = 128
TILE = CAP * PARTS
GROUPS = 4


def rms_scale(values, gain):
    return values * lax.rsqrt(jnp.mean(values * values, axis=-1, keepdims=True) + EPS) * gain


def unit_rows(values):
    return values * lax.rsqrt(jnp.sum(values * values, axis=-1, keepdims=True) + EPS)


def hop(slot, ring_z):
    i, dy = slot // RING_Y, slot % RING_Y
    dz = (i % 2) * ((i + 1) // 2) + (1 - i % 2) * ((ring_z - i // 2) % ring_z)
    return dz, dy


def iota(shape, dim):
    return lax.broadcasted_iota(jnp.int32, shape, dim)


def exchange_kernel(
    lanes, groups, partial_ref, tokens_ref, routes_ref, rw_ref, gain_ref, gate_hbm, up_hbm, down_hbm, out_ref,
    branch, packed, rows, wgate, wup, wdown, ysend, yrecv, gathered, back, resid_keep,
    local_sem, swap_send, swap_recv, b_send, b_recv, c_send, c_recv, d_send, d_recv, f_send, f_recv, g_send, g_recv,
):
    ring_z = groups // (RING_Y * CORES)
    plane = ring_z * RING_Y
    per_group = plane // GROUPS
    tp = lax.axis_index("tp")
    ep = lax.axis_index("ep")
    core = ep % CORES
    y = (ep // CORES) % RING_Y
    z = ep // (CORES * RING_Y)
    width = partial_ref.shape[1] // lanes

    def at(zz, yy):
        return (zz * RING_Y + yy) * CORES + core

    def forward(slot):
        dz, dy = hop(slot, ring_z)
        return (z + dz) % ring_z, (y + dy) % RING_Y

    def backward(slot):
        dz, dy = hop(slot, ring_z)
        return (z + ring_z - dz) % ring_z, (y + RING_Y - dy) % RING_Y

    partner = ep + 1 - 2 * core

    weights = ((gate_hbm, wgate), (up_hbm, wup), (down_hbm, wdown))
    loads = [pltpu.make_async_copy(src.at[0], dst.at[0], local_sem.at[i]) for i, (src, dst) in enumerate(weights)]
    for load in loads:
        load.start()

    barrier = pltpu.get_barrier_semaphore()
    pl.semaphore_signal(barrier, inc=1, device_id=(partner, tp), device_id_type=MESH)
    for dx in range(1, lanes):
        pl.semaphore_signal(barrier, inc=1, device_id=(ep, (tp + dx) % lanes), device_id_type=MESH)

    @pl.loop(1, plane)
    def _(slot):
        zz, yy = forward(slot)
        pl.semaphore_signal(barrier, inc=1, device_id=(at(zz, yy), tp), device_id_type=MESH)

    pl.semaphore_wait(barrier, plane - 1 + lanes - 1 + 1)

    sums = []
    for dx in range(1, lanes):
        to = (tp + dx) % lanes
        copy = pltpu.make_async_remote_copy(
            src_ref=partial_ref.at[:, pl.ds(pl.multiple_of(to * width, LANE), width)],
            dst_ref=branch.at[dx - 1],
            send_sem=b_send.at[dx - 1],
            recv_sem=b_recv.at[dx - 1],
            device_id=(ep, to),
            device_id_type=MESH,
        )
        copy.start()
        sums.append(copy)

    swaps = [
        pltpu.make_async_remote_copy(
            src_ref=src.at[0], dst_ref=dst.at[1], send_sem=swap_send.at[i], recv_sem=swap_recv.at[i],
            device_id=(partner, tp), device_id_type=MESH,
        )
        for i, (src, dst) in enumerate(weights)
    ]
    for swap in swaps:
        swap.start()

    experts = groups // 4
    seqs = routes_ref.shape[0]
    routes = routes_ref[...]
    rw = rw_ref[...]
    onehots = [(routes[:, k : k + 1] == iota((seqs, experts), 1)).astype(F32) for k in range(routes.shape[1])]
    earlier = (iota((seqs, seqs), 1) < iota((seqs, seqs), 0)).astype(F32)
    counts = jnp.dot(earlier, sum(onehots), preferred_element_type=F32)
    targets = []
    for k, onehot in enumerate(onehots):
        position = jnp.sum(counts * onehot, axis=1, keepdims=True).astype(jnp.int32)
        targets.append(routes[:, k : k + 1] * CAP + position)
    tall = [jnp.concatenate([t] * PARTS, axis=0) for t in targets]
    tall_w = [jnp.concatenate([rw[:, k : k + 1]] * PARTS, axis=0) for k in range(len(targets))]
    height = PARTS * seqs
    lane_id = iota((height, experts * TILE), 1)
    slot_of = (lane_id // TILE) * CAP + lane_id % CAP
    same_part = (lane_id % TILE) // CAP == iota((height, experts * TILE), 0) // seqs
    chosen = (tall[0] == slot_of) | (tall[1] == slot_of)
    select = (chosen & same_part).astype(F32).astype(BF16)

    mine = pl.ds(pl.multiple_of(tp * width, LANE), width)
    total = partial_ref[:, mine]
    for dx, copy in enumerate(sums):
        copy.wait_recv()
        total = total + branch[dx]
    resid = (tokens_ref[:, mine].astype(F32) + total.astype(BF16).astype(F32)).astype(BF16)
    resid_keep[...] = resid
    stacked = jnp.concatenate([resid[:, q * LANE : (q + 1) * LANE] for q in range(PARTS)], axis=0)
    picked = lax.dot_general(select, stacked, (((0,), (0,)), ((), ())), preferred_element_type=F32)
    packed[...] = picked.astype(BF16)

    def dispatch(slot):
        zz, yy = forward(slot)
        expert = zz * (RING_Y // 2) + yy // 2
        return pltpu.make_async_remote_copy(
            src_ref=packed.at[pl.ds(pl.multiple_of(expert * TILE, TILE), TILE), :],
            dst_ref=rows.at[tp, pl.ds(pl.multiple_of(slot * TILE, TILE), TILE), :],
            send_sem=c_send,
            recv_sem=c_recv.at[slot // per_group],
            device_id=(at(zz, yy), tp),
            device_id_type=MESH,
        )

    @pl.loop(1, plane)
    def _(slot):
        dispatch(slot).start()

    own_expert = z * (RING_Y // 2) + y // 2
    rows[tp, 0:TILE, :] = packed[pl.ds(pl.multiple_of(own_expert * TILE, TILE), TILE), :]

    def landed(ref, send_sem, recv_sem):
        return pltpu.make_async_remote_copy(
            src_ref=ref, dst_ref=ref, send_sem=send_sem, recv_sem=recv_sem, device_id=(partner, tp), device_id_type=MESH
        )

    spreads = []
    for g in range(GROUPS):
        first, last = g * per_group * TILE, (g + 1) * per_group * TILE
        fresh = max(first, TILE)
        landed(rows.at[tp, fresh:last, :], c_send, c_recv.at[g]).wait_recv()
        for dx in range(1, lanes):
            copy = pltpu.make_async_remote_copy(
                src_ref=rows.at[tp, first:last, :],
                dst_ref=rows.at[tp, first:last, :],
                send_sem=d_send.at[g, dx - 1],
                recv_sem=d_recv.at[g, dx - 1],
                device_id=(ep, (tp + dx) % lanes),
                device_id_type=MESH,
            )
            copy.start()
            spreads.append((g, dx, first, last, copy))

    lane_id = iota((height, plane * TILE), 1)
    dz, dy = hop(lane_id // TILE, ring_z)
    expert = ((z + dz) % ring_z) * (RING_Y // 2) + ((y + dy) % RING_Y) // 2
    slot_of = expert * CAP + lane_id % CAP
    same_part = (lane_id % TILE) // CAP == iota((height, plane * TILE), 0) // seqs
    combine = jnp.zeros((height, plane * TILE), F32)
    for target, weight in zip(tall, tall_w):
        combine = combine + jnp.where((target == slot_of) & same_part, weight, 0.0)

    many = 16
    span = many * TILE
    row_id, col_id = iota((span, span), 0), iota((span, span), 1)

    def shuffled(index):
        part, rest = index // (many * CAP), index % (many * CAP)
        return (rest // CAP) * TILE + part * CAP + rest % CAP

    sort = (shuffled(row_id) == col_id).astype(F32).astype(BF16)
    unsort = (shuffled(col_id) == row_id).astype(F32).astype(BF16)

    for g, dx, first, last, copy in spreads:
        source = (tp + lanes - dx) % lanes
        landed(rows.at[source, first:last, :], d_send.at[g, dx - 1], d_recv.at[g, dx - 1]).wait_recv()

    chunks = plane // many
    pieces = []
    for c in range(chunks):
        wide = jnp.concatenate([rows[x, c * span : (c + 1) * span, :] for x in range(lanes)], axis=1)
        ordered = jnp.dot(sort, wide, preferred_element_type=F32)
        high = many * CAP
        pieces.append(
            jnp.concatenate(
                [ordered[q * high : (q + 1) * high, x * LANE : (x + 1) * LANE] for x in range(lanes) for q in range(PARTS)],
                axis=1,
            )
        )
    arrived = jnp.concatenate(pieces, axis=0)
    ffn_in = rms_scale(arrived, gain_ref[...]).astype(BF16)

    for load in loads:
        load.wait()
    for swap in swaps:
        swap.wait_recv()
    hidden = []
    for s in range(CORES):
        gated = jnp.dot(ffn_in, wgate[s], preferred_element_type=F32)
        lifted = jnp.dot(ffn_in, wup[s], preferred_element_type=F32)
        hidden.append((jax.nn.silu(gated) * lifted).astype(BF16))

    gives = []
    high = many * CAP
    for c in range(chunks):
        part = sum(
            jnp.dot(hidden[s][c * high : (c + 1) * high], wdown[s], preferred_element_type=F32) for s in range(CORES)
        ).astype(BF16)
        tall_part = jnp.concatenate(
            [
                jnp.concatenate([part[:, (x * PARTS + q) * LANE : (x * PARTS + q + 1) * LANE] for x in range(lanes)], axis=1)
                for q in range(PARTS)
            ],
            axis=0,
        )
        split = jnp.dot(unsort, tall_part, preferred_element_type=F32).astype(BF16)
        for x in range(lanes):
            ysend[x, c * span : (c + 1) * span, :] = split[:, x * LANE : (x + 1) * LANE]
        for dx in range(1, lanes):
            to = (tp + dx) % lanes
            copy = pltpu.make_async_remote_copy(
                src_ref=ysend.at[to, c * span : (c + 1) * span, :],
                dst_ref=yrecv.at[dx - 1, c * span : (c + 1) * span, :],
                send_sem=f_send.at[c, dx - 1],
                recv_sem=f_recv.at[c, dx - 1],
                device_id=(ep, to),
                device_id_type=MESH,
            )
            copy.start()
            gives.append(copy)

    def give_back(slot):
        zz, yy = backward(slot)
        return pltpu.make_async_remote_copy(
            src_ref=gathered.at[pl.ds(pl.multiple_of(slot * TILE, TILE), TILE), :],
            dst_ref=back.at[pl.ds(pl.multiple_of(slot * TILE, TILE), TILE), :],
            send_sem=g_send,
            recv_sem=g_recv,
            device_id=(at(zz, yy), tp),
            device_id_type=MESH,
        )

    for c in range(chunks):
        own = ysend[tp, c * span : (c + 1) * span, :].astype(F32)
        for dx in range(1, lanes):
            gives[c * (lanes - 1) + dx - 1].wait_recv()
            own = own + yrecv[dx - 1, c * span : (c + 1) * span, :].astype(F32)
        gathered[c * span : (c + 1) * span, :] = own.astype(BF16)

        @pl.loop(max(1, c * many), (c + 1) * many)
        def _(slot):
            give_back(slot).start()

        if c == 0:
            back[0:TILE, :] = gathered[0:TILE, :]

    landed(back.at[TILE : plane * TILE, :], g_send, g_recv).wait_recv()
    moe = jnp.dot(combine, back[...].astype(F32), preferred_element_type=F32, precision=lax.Precision.HIGHEST)
    moe = jnp.concatenate([moe[q * seqs : (q + 1) * seqs] for q in range(PARTS)], axis=1)
    out_ref[...] = (resid_keep[...].astype(F32) + moe).astype(BF16)

    for copy in sums:
        copy.wait_send()
    for swap in swaps:
        swap.wait_send()
    landed(back.at[TILE : plane * TILE, :], c_send, g_recv).wait_send()
    for _, _, _, _, copy in spreads:
        copy.wait_send()
    for copy in gives:
        copy.wait_send()
    landed(back.at[TILE : plane * TILE, :], g_send, g_recv).wait_send()


def exchange(partial_out, tokens, routes, route_weight, ffn_gain, expert_gate, expert_up, expert_down):
    lanes, groups = lax.axis_size("tp"), lax.axis_size("ep")
    seqs, model = tokens.shape
    width = model // lanes
    plane = groups // CORES
    chunks = plane // 16
    hidden = expert_gate.shape[2]
    vmem, anywhere = pl.BlockSpec(memory_space=pltpu.VMEM), pl.BlockSpec(memory_space=pl.ANY)
    dma = pltpu.SemaphoreType.DMA
    return pl.pallas_call(
        functools.partial(exchange_kernel, lanes, groups),
        name="exchange",
        out_shape=jax.ShapeDtypeStruct((seqs, width), BF16),
        in_specs=[vmem] * 5 + [anywhere] * 3,
        out_specs=vmem,
        scratch_shapes=[
            pltpu.VMEM((lanes - 1, seqs, width), F32),
            pltpu.VMEM((groups // 4 * TILE, LANE), BF16),
            pltpu.VMEM((lanes, plane * TILE, LANE), BF16),
            pltpu.VMEM((CORES, model, hidden), BF16),
            pltpu.VMEM((CORES, model, hidden), BF16),
            pltpu.VMEM((CORES, hidden, model), BF16),
            pltpu.VMEM((lanes, plane * TILE, LANE), BF16),
            pltpu.VMEM((lanes - 1, plane * TILE, LANE), BF16),
            pltpu.VMEM((plane * TILE, LANE), BF16),
            pltpu.VMEM((plane * TILE, LANE), BF16),
            pltpu.VMEM((seqs, width), BF16),
            dma((3,)),
            dma((3,)),
            dma((3,)),
            dma((lanes - 1,)),
            dma((lanes - 1,)),
            dma,
            dma((GROUPS,)),
            dma((GROUPS, lanes - 1)),
            dma((GROUPS, lanes - 1)),
            dma((chunks, lanes - 1)),
            dma((chunks, lanes - 1)),
            dma,
            dma,
        ],
        compiler_params=pltpu.CompilerParams(
            collective_id=0, has_side_effects=True, vmem_limit_bytes=32 * 1024 * 1024
        ),
    )(partial_out, tokens, routes, route_weight, ffn_gain.reshape(1, -1), expert_gate, expert_up, expert_down)


def local(
    tokens,
    recur_state,
    attn_gain,
    query_weight,
    key_weight,
    value_weight,
    outgate_weight,
    beta_weight,
    decay_weight,
    decay_rate,
    head_gain,
    output_weight,
    ffn_gain,
    routes,
    route_weight,
    expert_gate,
    expert_up,
    expert_down,
):
    highest = lax.Precision.HIGHEST
    seq_count = tokens.shape[0]
    heads_here = recur_state.shape[1]
    head_size = recur_state.shape[2]
    lane_index = lax.axis_index("tp")
    normed = rms_scale(tokens.astype(F32), attn_gain).astype(BF16)
    qproj = jnp.dot(normed, query_weight, preferred_element_type=F32).astype(BF16)
    kproj = jnp.dot(normed, key_weight, preferred_element_type=F32).astype(BF16)
    vproj = jnp.dot(normed, value_weight, preferred_element_type=F32).astype(BF16)
    zproj = jnp.dot(normed, outgate_weight, preferred_element_type=F32).astype(BF16)
    first_head = lane_index * heads_here
    own_beta = lax.dynamic_slice_in_dim(beta_weight, first_head, heads_here, 1)
    own_decay = lax.dynamic_slice_in_dim(decay_weight, first_head, heads_here, 1)
    own_rate = lax.dynamic_slice_in_dim(decay_rate, first_head, heads_here, 0)
    strength = jax.nn.sigmoid(jnp.dot(normed, own_beta, preferred_element_type=F32))
    fading = jnp.exp(-own_rate * jax.nn.softplus(jnp.dot(normed, own_decay, preferred_element_type=F32)))

    def split_heads(proj):
        return proj.astype(F32).reshape(seq_count, heads_here, head_size)

    query = unit_rows(jax.nn.silu(split_heads(qproj))) * head_size ** (-0.5)
    keyvec = unit_rows(jax.nn.silu(split_heads(kproj)))
    value = jax.nn.silu(split_heads(vproj))
    recall = jnp.einsum("thd,thde->the", keyvec, recur_state, precision=highest)
    written = (strength[..., None] * keyvec)[..., :, None] * (value - fading[..., None] * recall)[..., None, :]
    new_state = fading[..., None, None] * recur_state + written
    readout = jnp.einsum("thd,thde->the", query, new_state, precision=highest)
    headed = (
        (rms_scale(readout, head_gain) * jax.nn.silu(split_heads(zproj)))
        .reshape(seq_count, heads_here * head_size)
        .astype(BF16)
    )
    partial_out = jnp.dot(headed, output_weight, preferred_element_type=F32)
    mixed = exchange(partial_out, tokens, routes, route_weight, ffn_gain, expert_gate, expert_up, expert_down)
    return (mixed, new_state)


def solution(mesh):
    return jax.shard_map(
        local,
        mesh=mesh,
        in_specs=(
            P("ep", None),
            P("ep", "tp", None, None),
            P(),
            P(None, "tp"),
            P(None, "tp"),
            P(None, "tp"),
            P(None, "tp"),
            P(),
            P(),
            P(),
            P(),
            P("tp", None),
            P(),
            P("ep", None),
            P("ep", None),
            P("ep", None, "tp"),
            P("ep", None, "tp"),
            P("ep", "tp", None),
        ),
        out_specs=(P("ep", "tp"), P("ep", "tp", None, None)),
        check_vma=False,
    )
```

time: 116 us -> 62.5 us (0.54)
  the two profiles are of different devices: /device:TPU:1 before, /device:TPU:32 now
where the time goes in v1:
time: 62.5 us; the launch traced here: 62.2 us
  Pallas kernels  42.6 us (68%)
  matrix products  12.8 us (20%)
  other arithmetic  3.22 us (5%)
  local copies, waits for them, and re-layouts  2.65 us (4%)
  between operations  0.88 us (1%)
    pallas_call x1, Pallas kernels, exchange(): pl.pallas_call(functools.partial(exchange_kernel, lanes, groups), name='e...  42.6 us
    dot_general x1, matrix products, local(): recall = jnp.einsum('thd,thde->the', keyvec, recur_state, precision=highest)  3.5 us
    unnamed x25, local copies, waits for them, and re-layouts  2.42 us
    dot_general x1, matrix products, local(): readout = jnp.einsum('thd,thde->the', query, new_state, precision=highest)  1.86 us
    dot_general x1, matrix products, local(): jnp.dot(normed, outgate_weight, preferred_element_type=F32).astype(BF16)  1.72 us
    dot_general x1, matrix products, local(): kproj = jnp.dot(normed, key_weight, preferred_element_type=F32).astype(BF16)  1.56 us
    dot_general x1, matrix products, local(): jnp.dot(normed, query_weight, preferred_element_type=F32).astype(BF16)  1.51 us

profile of v1, /device:TPU:32, one launch (start us, length us, event | category | flops | bytes accessed | tf_op | source)
XLA Modules:
  0.0 62.2 jit_solution(12667866163922027415)
XLA Ops:
  0.7 0.8 %dynamic-slice_negate_fusion = f32[2]{0:T(128)S(1)} fusion(f32[8]{0:T(128)} %param.27, s32[]{:T(128)S(6)} %select_n.9), kind=kLoop, calls=%fused_computation.43 | loop fusion | flops 2 | bytes 20 | tf_op jit(solution)/shard_map/neg | solution.py:384
  1.5 1.0 %fusion.7 = f32[16]{0:T(128)S(1)} fusion(bf16[16,2048]{1,0:T(8,128)(2,1)} %tokens_ref.1), kind=kLoop, calls=%fused_computation.15 | loop fusion | flops 98288 | bytes 65600 | tf_op jit(solution)/shard_map/reduce_sum | solution.py:24
  2.5 1.1 %fusion.20 = f32[16,2]{0,1:T(2,128)S(1)} fusion(bf16[2048,8]{0,1:T(8,128)(2,1)} %param.26, s32[]{:T(128)S(6)} %select_n.9, f32[2]{0:T(128)S(1)} %dynamic-slice_negate_fusion, bf16[16,2048]{1,0:T(8,128)(2,1)} %tokens_ref.1, f32[2048]{0:T(1024)} %param.20, f32[16]{0:T(128)S(1)} %add_rsqrt_fusion.3), kind=kOutput, calls=%fused_computation.42 | convolution fusion | flops 262368 | bytes 82124 | tf_op jit(solution)/shard_map/dot_general | solution.py:384
  3.6 1.1 %fusion.6 = f32[16,2]{0,1:T(2,128)S(1)} fusion(bf16[2048,8]{0,1:T(8,128)(2,1)} %param.25, s32[]{:T(128)S(6)} %select_n.9, bf16[16,2048]{1,0:T(8,128)(2,1)} %tokens_ref.1, f32[2048]{0:T(1024)} %param.20, f32[16]{0:T(128)S(1)} %add_rsqrt_fusion.3), kind=kOutput, calls=%fused_computation.12 | convolution fusion | flops 262240 | bytes 82116 | tf_op jit(solution)/shard_map/dot_general | solution.py:383
  4.6 0.1 copy.20
  4.8 0.8 %copy.23.routes_ref = s32[16,2]{1,0:T(8,128)S(1)} copy(s32[16,2]{0,1:T(2,128)} %param.31) | data formatting | bytes 256 | tf_op args[13]
  5.6 0.8 %copy.24.rw_ref = f32[16,2]{1,0:T(8,128)S(1)} copy(f32[16,2]{0,1:T(2,128)} %param.32) | data formatting | bytes 256 | tf_op args[14]
  6.3 1.6 %fusion.2 = f32[16,256]{1,0:T(8,128)S(1)} fusion(bf16[2048,256]{1,0:T(8,128)(2,1)} %param.22, bf16[16,2048]{1,0:T(8,128)(2,1)} %tokens_ref.1, f32[2048]{0:T(1024)} %param.20, f32[16]{0:T(128)S(1)} %add_rsqrt_fusion.3), kind=kOutput, calls=%fused_computation.6 | convolution fusion | flops 16916480 | bytes 1138752 | tf_op jit(solution)/shard_map/dot_general | solution.py:376
  7.9 0.1 multiply_reduce_fusion.1
  8.0 0.1 broadcast_multiply_fusion.1
  8.1 3.5 %fusion.31 = f32[16,2,1,128]{3,2,1,0:T(1,128)S(1)} fusion(f32[16,2,128,1]{2,3,1,0:T(1,128)S(1)} %bitcast.29, f32[16,2,128,128]{3,2,1,0:T(8,128)} %param.19), kind=kOutput, calls=%fused_computation.47 | convolution fusion | flops 6291456 | bytes 2129920 | tf_op jit(solution)/shard_map/thd,thde->the/dot_general | solution.py:392
  11.7 0.3 fusion.1
  12.0 0.1 fusion.10
  12.1 1.7 %fusion = f32[16,256]{1,0:T(8,128)S(1)} fusion(bf16[2048,256]{1,0:T(8,128)(2,1)} %param.24, bf16[16,2048]{1,0:T(8,128)(2,1)S(1)} %copy-done.1, f32[2048]{0:T(1024)S(1)} %copy-done.9, f32[16]{0:T(128)S(1)} %add_rsqrt_fusion.3), kind=kOutput, calls=%fused_computation.2 | convolution fusion | flops 16916480 | bytes 1138752 | tf_op jit(solution)/shard_map/dot_general | solution.py:378
  13.8 1.5 %fusion.3 = f32[16,256]{1,0:T(8,128)S(1)} fusion(bf16[2048,256]{1,0:T(8,128)(2,1)} %param.21, bf16[16,2048]{1,0:T(8,128)(2,1)S(1)} %copy-done.1, f32[2048]{0:T(1024)S(1)} %copy-done.9, f32[16]{0:T(128)S(1)} %add_rsqrt_fusion.3), kind=kOutput, calls=%fused_computation.8 | convolution fusion | flops 16916480 | bytes 1138752 | tf_op jit(solution)/shard_map/dot_general | solution.py:375
  15.3 0.1 multiply_reduce_fusion.2
  15.6 0.7 %multiply_add_fusion = f32[16,2,128,128]{3,2,1,0:T(8,128)S(1)} fusion(f32[16,2,128,128]{3,2,1,0:T(8,128)S(1)} %copy-done.6, f32[16,2,128]{2,1,0:T(2,128)S(1)} %fusion.10, f32[16,2,128]{2,1,0:T(2,128)S(1)} %get-tuple-element.2, f32[16,2]{1,0:T(8,128)S(1)} %copy.20), kind=kLoop, calls=%fused_computation | loop fusion | flops 1572864 | bytes 4227200 | tf_op jit(solution)/shard_map/add | solution.py:394
  16.4 1.9 %fusion.32 = f32[16,2,1,128]{3,2,1,0:T(1,128)S(1)} fusion(f32[16,2,128,1]{2,3,1,0:T(1,128)S(1)} %bitcast.28, f32[16,2,128,128]{3,2,1,0:T(8,128)S(1)} %multiply_add_fusion), kind=kOutput, calls=%fused_computation.48 | convolution fusion | flops 6291456 | bytes 2129920 | tf_op jit(solution)/shard_map/thd,thde->the/dot_general | solution.py:395
  18.3 0.1 multiply_reduce_fusion
  18.4 0.1 fusion.12
  18.5 0.3 fusion.13.partial_ref
  18.7 0.2 copy-done.4
  19.0 42.6 %exchange.1 = bf16[16,512]{1,0:T(8,128)(2,1)S(1)} custom-call(f32[16,2048]{1,0:T(8,128)S(1)} %fusion.13.partial_ref, bf16[16,2048]{1,0:T(8,128)(2,1)S(1)} %copy-done.1, s32[16,2]{1,0:T(8,128)S(1)} %copy.23.routes_ref, f32[16,2]{1,0:T(8,128)S(1)} %copy.24.rw_ref, f32[1,2048]{1,0:T(1,128)S(1)} %bitcast.24, bf16[1,2048,256]{2,1,0:T(8,128)(2,1)S(1)} %copy-done.2, ...), custom_call_target="tpu_custom_call" | custom-call | tf_op jit(solution)/shard_map/exchange/pallas_call | solution.py:311
  61.6 0.6 copy.35
  (31 shorter events, 0.3 us)
Async XLA Ops:
  0.6 17.8 %copy-start = (bf16[256,2048]{1,0:T(8,128)(2,1)S(1)}, bf16[256,2048]{1,0:T(8,128)(2,1)}, u32[]{:S(2)}) copy-start(bf16[256,2048]{1,0:T(8,128)(2,1)} %param.29) | copy-start | bytes 3145732
  0.6 11.0 %copy-start.1 = (bf16[16,2048]{1,0:T(8,128)(2,1)S(1)}, bf16[16,2048]{1,0:T(8,128)(2,1)}, u32[]{:S(2)}) copy-start(bf16[16,2048]{1,0:T(8,128)(2,1)} %tokens_ref.1) | copy-start | bytes 196612
  0.7 11.0 %copy-start.9 = (f32[2048]{0:T(1024)S(1)}, f32[2048]{0:T(1024)}, u32[]{:S(2)}) copy-start(f32[2048]{0:T(1024)} %param.20) | copy-start | bytes 24580
  7.9 3.8 %copy-start.8 = (bf16[2048,256]{1,0:T(8,128)(2,1)S(1)}, bf16[2048,256]{1,0:T(8,128)(2,1)}, u32[]{:S(2)}) copy-start(bf16[2048,256]{1,0:T(8,128)(2,1)} %param.23) | copy-start | bytes 3145732
  11.6 3.9 %copy-start.6 = (f32[16,2,128,128]{3,2,1,0:T(8,128)S(1)}, f32[16,2,128,128]{3,2,1,0:T(8,128)}, u32[]{:S(2)}) copy-start(f32[16,2,128,128]{3,2,1,0:T(8,128)} %param.19) | copy-start | bytes 6291460
  15.6 2.8 %copy-start.10 = (f32[128]{0:T(128)S(1)}, f32[128]{0:T(128)}, u32[]{:S(2)}) copy-start(f32[128]{0:T(128)} %param.28) | copy-start | bytes 1540
  16.3 45.2 %copy-start.7 = (f32[16,2,128,128]{3,2,1,0:T(8,128)}, f32[16,2,128,128]{3,2,1,0:T(8,128)S(1)}, u32[]{:S(2)}) copy-start(f32[16,2,128,128]{3,2,1,0:T(8,128)S(1)} %multiply_add_fusion) | copy-start | bytes 6291460
  16.3 2.4 %copy-start.2 = (bf16[1,2048,256]{2,1,0:T(8,128)(2,1)S(1)}, bf16[1,2048,256]{2,1,0:T(8,128)(2,1)}, u32[]{:S(2)}) copy-start(bf16[1,2048,256]{2,1,0:T(8,128)(2,1)} %gate_hbm.1) | copy-start | bytes 3145732
  16.3 2.4 %copy-start.3 = (bf16[1,2048,256]{2,1,0:T(8,128)(2,1)S(1)}, bf16[1,2048,256]{2,1,0:T(8,128)(2,1)}, u32[]{:S(2)}) copy-start(bf16[1,2048,256]{2,1,0:T(8,128)(2,1)} %up_hbm.1) | copy-start | bytes 3145732
  16.4 2.6 %copy-start.4 = (bf16[1,256,2048]{2,1,0:T(8,128)(2,1)S(1)}, bf16[1,256,2048]{2,1,0:T(8,128)(2,1)}, u32[]{:S(2)}) copy-start(bf16[1,256,2048]{2,1,0:T(8,128)(2,1)} %down_hbm.1) | copy-start | bytes 3145732
  16.4 2.6 %copy-start.5 = (f32[2048]{0:T(1024)S(1)}, f32[2048]{0:T(1024)}, u32[]{:S(2)}) copy-start(f32[2048]{0:T(1024)} %param.30) | copy-start | bytes 24580

commit v2 on v1

--- a/solution.py
+++ b/solution.py
@@ -11,6 +11,7 @@
 MESH = pl.DeviceIdType.MESH
 F32 = jnp.float32
 BF16 = jnp.bfloat16
+HIGHEST = lax.Precision.HIGHEST
 CORES = 2
 RING_Y = 4
 CAP = 4
@@ -18,6 +19,7 @@
 LANE = 128
 TILE = CAP * PARTS
 GROUPS = 4
+STATE_CHUNKS = 4
 
 
 def rms_scale(values, gain):
@@ -36,6 +38,115 @@
 
 def iota(shape, dim):
     return lax.broadcasted_iota(jnp.int32, shape, dim)
+
+
+def mixer_kernel(
+    heads, tokens_ref, gain_ref, beta_ref, decay_ref, rate_ref, head_gain_ref, q_hbm, k_hbm, v_hbm, z_hbm, o_hbm, state_hbm,
+    partial_ref, new_hbm, wq, wk, wv, wz, wo, state, read, load_sem, state_sem, out_sem,
+):
+    tp = lax.axis_index("tp")
+    seqs = tokens_ref.shape[0]
+    loads = {
+        name: pltpu.make_async_copy(src, dst, load_sem.at[i])
+        for i, (name, src, dst) in enumerate(
+            (("k", k_hbm, wk), ("q", q_hbm, wq), ("v", v_hbm, wv), ("z", z_hbm, wz), ("o", o_hbm, wo))
+        )
+    }
+    step = seqs // STATE_CHUNKS
+    reads = [
+        pltpu.make_async_copy(state_hbm.at[pl.ds(c * step, step)], state.at[pl.ds(c * step, step)], state_sem.at[c])
+        for c in range(STATE_CHUNKS)
+    ]
+    for name in "kqv":
+        loads[name].start()
+    for read_in in reads:
+        read_in.start()
+    for name in "zo":
+        loads[name].start()
+
+    normed = rms_scale(tokens_ref[...].astype(F32), gain_ref[...]).astype(BF16)
+
+    def by_head(weight_ref):
+        return lax.dot_general(normed, weight_ref[...], (((1,), (1,)), ((), ())), preferred_element_type=F32)
+
+    strength = jax.nn.sigmoid(by_head(beta_ref))
+    fading = jnp.exp(-rate_ref[...] * jax.nn.softplus(by_head(decay_ref)))
+
+    def own_head(values, h):
+        chosen = iota(values.shape, 1) == tp * heads + h
+        column = jnp.sum(jnp.where(chosen, values, 0.0), axis=1, keepdims=True)
+        return jnp.broadcast_to(column, (seqs, LANE))
+
+    strengths = [own_head(strength, h) for h in range(heads)]
+    fadings = [own_head(fading, h) for h in range(heads)]
+
+    def project(name, weight):
+        loads[name].wait()
+        proj = jnp.dot(normed, weight[...], preferred_element_type=F32).astype(BF16).astype(F32)
+        return [jax.nn.silu(proj[:, h * LANE : (h + 1) * LANE]) for h in range(heads)]
+
+    keys = [unit_rows(k) for k in project("k", wk)]
+    queries = [unit_rows(q) * LANE ** (-0.5) for q in project("q", wq)]
+    filler = [jnp.zeros((LANE - 2 * heads * seqs, LANE), F32)]
+    columns = jnp.concatenate(keys + queries + filler, axis=0).T
+    values = project("v", wv)
+
+    writes = []
+    for c in range(STATE_CHUNKS):
+        reads[c].wait()
+        for t in range(c * step, (c + 1) * step):
+            for h in range(heads):
+                j = h * seqs + t
+                key, query = columns[:, j : j + 1], columns[:, heads * seqs + j : heads * seqs + j + 1]
+                fade = fadings[h][t : t + 1]
+                old = state[t, h]
+                recall = jnp.sum(old * key, axis=0, keepdims=True)
+                delta = strengths[h][t : t + 1] * (values[h][t : t + 1] - fade * recall)
+                new = fade * old + key * delta
+                state[t, h] = new
+                read[t : t + 1, h * LANE : (h + 1) * LANE] = jnp.sum(new * query, axis=0, keepdims=True)
+        write = pltpu.make_async_copy(state.at[pl.ds(c * step, step)], new_hbm.at[pl.ds(c * step, step)], out_sem.at[c])
+        write.start()
+        writes.append(write)
+
+    gates = project("z", wz)
+    headed = [
+        (rms_scale(read[:, h * LANE : (h + 1) * LANE], head_gain_ref[...]) * gates[h]).astype(BF16) for h in range(heads)
+    ]
+    loads["o"].wait()
+    partial_ref[...] = jnp.dot(jnp.concatenate(headed, axis=1), wo[...], preferred_element_type=F32)
+    for write in writes:
+        write.wait()
+
+
+def mixer(
+    tokens, recur_state, attn_gain, query_weight, key_weight, value_weight, outgate_weight, beta_weight, decay_weight,
+    decay_rate, head_gain, output_weight,
+):
+    seqs, model = tokens.shape
+    heads, size = recur_state.shape[1:3]
+    vmem, anywhere = pl.BlockSpec(memory_space=pltpu.VMEM), pl.BlockSpec(memory_space=pltpu.HBM)
+    dma = pltpu.SemaphoreType.DMA
+    return pl.pallas_call(
+        functools.partial(mixer_kernel, heads),
+        name="mixer",
+        out_shape=(jax.ShapeDtypeStruct((seqs, model), F32), jax.ShapeDtypeStruct(recur_state.shape, F32)),
+        in_specs=[vmem] * 6 + [anywhere] * 6,
+        out_specs=(vmem, anywhere),
+        scratch_shapes=[pltpu.VMEM((model, heads * size), BF16)] * 4
+        + [
+            pltpu.VMEM((heads * size, model), BF16),
+            pltpu.VMEM(recur_state.shape, F32),
+            pltpu.VMEM((seqs, heads * size), F32),
+            dma((5,)),
+            dma((STATE_CHUNKS,)),
+            dma((STATE_CHUNKS,)),
+        ],
+        compiler_params=pltpu.CompilerParams(vmem_limit_bytes=24 * 1024 * 1024),
+    )(
+        tokens, attn_gain.reshape(1, -1), beta_weight.T, decay_weight.T, decay_rate.reshape(1, -1), head_gain.reshape(1, -1),
+        query_weight, key_weight, value_weight, outgate_weight, output_weight, recur_state,
+    )
 
 
 def exchange_kernel(
@@ -108,9 +219,14 @@
         swap.start()
 
     experts = groups // 4
-    seqs = routes_ref.shape[0]
-    routes = routes_ref[...]
-    rw = rw_ref[...]
+    seqs = routes_ref.shape[1]
+    eye = (iota((seqs, seqs), 0) == iota((seqs, seqs), 1)).astype(F32)
+
+    def upright(flat):
+        return lax.dot_general(eye, flat, (((1,), (1,)), ((), ())), preferred_element_type=F32, precision=HIGHEST)
+
+    routes = upright(routes_ref[...].astype(F32)).astype(jnp.int32)
+    rw = upright(rw_ref[...])
     onehots = [(routes[:, k : k + 1] == iota((seqs, experts), 1)).astype(F32) for k in range(routes.shape[1])]
     earlier = (iota((seqs, seqs), 1) < iota((seqs, seqs), 0)).astype(F32)
     counts = jnp.dot(earlier, sum(onehots), preferred_element_type=F32)
@@ -283,7 +399,7 @@
             back[0:TILE, :] = gathered[0:TILE, :]
 
     landed(back.at[TILE : plane * TILE, :], g_send, g_recv).wait_recv()
-    moe = jnp.dot(combine, back[...].astype(F32), preferred_element_type=F32, precision=lax.Precision.HIGHEST)
+    moe = jnp.dot(combine, back[...].astype(F32), preferred_element_type=F32, precision=HIGHEST)
     moe = jnp.concatenate([moe[q * seqs : (q + 1) * seqs] for q in range(PARTS)], axis=1)
     out_ref[...] = (resid_keep[...].astype(F32) + moe).astype(BF16)
 
@@ -306,7 +422,7 @@
     plane = groups // CORES
     chunks = plane // 16
     hidden = expert_gate.shape[2]
-    vmem, anywhere = pl.BlockSpec(memory_space=pltpu.VMEM), pl.BlockSpec(memory_space=pl.ANY)
+    vmem, anywhere = pl.BlockSpec(memory_space=pltpu.VMEM), pl.BlockSpec(memory_space=pltpu.HBM)
     dma = pltpu.SemaphoreType.DMA
     return pl.pallas_call(
         functools.partial(exchange_kernel, lanes, groups),
@@ -343,7 +459,7 @@
         compiler_params=pltpu.CompilerParams(
             collective_id=0, has_side_effects=True, vmem_limit_bytes=32 * 1024 * 1024
         ),
-    )(partial_out, tokens, routes, route_weight, ffn_gain.reshape(1, -1), expert_gate, expert_up, expert_down)
+    )(partial_out, tokens, routes.T, route_weight.T, ffn_gain.reshape(1, -1), expert_gate, expert_up, expert_down)
 
 
 def local(
@@ -366,39 +482,10 @@
     expert_up,
     expert_down,
 ):
-    highest = lax.Precision.HIGHEST
-    seq_count = tokens.shape[0]
-    heads_here = recur_state.shape[1]
-    head_size = recur_state.shape[2]
-    lane_index = lax.axis_index("tp")
-    normed = rms_scale(tokens.astype(F32), attn_gain).astype(BF16)
-    qproj = jnp.dot(normed, query_weight, preferred_element_type=F32).astype(BF16)
-    kproj = jnp.dot(normed, key_weight, preferred_element_type=F32).astype(BF16)
-    vproj = jnp.dot(normed, value_weight, preferred_element_type=F32).astype(BF16)
-    zproj = jnp.dot(normed, outgate_weight, preferred_element_type=F32).astype(BF16)
-    first_head = lane_index * heads_here
-    own_beta = lax.dynamic_slice_in_dim(beta_weight, first_head, heads_here, 1)
-    own_decay = lax.dynamic_slice_in_dim(decay_weight, first_head, heads_here, 1)
-    own_rate = lax.dynamic_slice_in_dim(decay_rate, first_head, heads_here, 0)
-    strength = jax.nn.sigmoid(jnp.dot(normed, own_beta, preferred_element_type=F32))
-    fading = jnp.exp(-own_rate * jax.nn.softplus(jnp.dot(normed, own_decay, preferred_element_type=F32)))
-
-    def split_heads(proj):
-        return proj.astype(F32).reshape(seq_count, heads_here, head_size)
-
-    query = unit_rows(jax.nn.silu(split_heads(qproj))) * head_size ** (-0.5)
-    keyvec = unit_rows(jax.nn.silu(split_heads(kproj)))
-    value = jax.nn.silu(split_heads(vproj))
-    recall = jnp.einsum("thd,thde->the", keyvec, recur_state, precision=highest)
-    written = (strength[..., None] * keyvec)[..., :, None] * (value - fading[..., None] * recall)[..., None, :]
-    new_state = fading[..., None, None] * recur_state + written
-    readout = jnp.einsum("thd,thde->the", query, new_state, precision=highest)
-    headed = (
-        (rms_scale(readout, head_gain) * jax.nn.silu(split_heads(zproj)))
-        .reshape(seq_count, heads_here * head_size)
-        .astype(BF16)
+    partial_out, new_state = mixer(
+        tokens, recur_state, attn_gain, query_weight, key_weight, value_weight, outgate_weight, beta_weight, decay_weight,
+        decay_rate, head_gain, output_weight,
     )
-    partial_out = jnp.dot(headed, output_weight, preferred_element_type=F32)
     mixed = exchange(partial_out, tokens, routes, route_weight, ffn_gain, expert_gate, expert_up, expert_down)
     return (mixed, new_state)
 

time: 62.5 us -> 61.5 us (0.984)
  matrix products: 12.8 us -> 0 us
  local copies, waits for them, and re-layouts: 2.65 us -> 12.7 us
  Pallas kernels: 42.6 us -> 47.5 us
  other arithmetic: 3.22 us -> 0 us
    dot_general x9 -> x0, matrix products: 12.8 us -> none  [the longest x1 3.5 us: local(): recall = jnp.einsum('thd,thde->the', keyvec, recur_state, precision=highest)]
    unnamed x25 -> x39, local copies, waits for them, and re-layouts: 2.42 us -> 12.7 us
    pallas_call x0 -> x1, Pallas kernels: none -> 4.73 us  [mixer(): pl.pallas_call(functools.partial(mixer_kernel, heads), name='mixer', out_...]
    reduce_sum x4 -> x0, other arithmetic: 1.27 us -> none  [the longest x2 1.06 us: rms_scale(): jnp.mean(values * values, axis=-1, keepdims=True) + EPS]
    neg x1 -> x0, other arithmetic: 0.82 us -> none  [local(): -own_rate]
    add x1 -> x0, other arithmetic: 0.74 us -> none  [local(): new_state = fading[..., None, None] * recur_state + written]
where the time goes in v2:
time: 61.5 us; the launch traced here: 61 us
  Pallas kernels  47.5 us (77%)
  local copies, waits for them, and re-layouts  12.7 us (21%)
  between operations  0.76 us (1%)
    pallas_call x1, Pallas kernels, exchange(): pl.pallas_call(functools.partial(exchange_kernel, lanes, groups), name='e...  42.8 us
    unnamed x39, local copies, waits for them, and re-layouts  12.7 us
    pallas_call x1, Pallas kernels, mixer(): pl.pallas_call(functools.partial(mixer_kernel, heads), name='mixer', out_...  4.73 us

profile of v2, /device:TPU:32, one launch (start us, length us, event | category | flops | bytes accessed | tf_op | source)
XLA Modules:
  0.0 61.0 jit_solution(17912177780451617440)
XLA Ops:
  0.6 0.0 copy-start
  0.6 1.6 %copy-done = f32[16,2,128,128]{3,2,1,0:T(8,128)S(1)} copy-done((f32[16,2,128,128]{3,2,1,0:T(8,128)S(1)}, f32[16,2,128,128]{3,2,1,0:T(8,128)}, u32[]{:S(2)}) %copy-start) | copy-done | bytes 2097176
  2.2 1.2 %copy-done.1 = bf16[2048,256]{1,0:T(8,128)(2,1)S(1)} copy-done((bf16[2048,256]{1,0:T(8,128)(2,1)S(1)}, bf16[2048,256]{1,0:T(8,128)(2,1)}, u32[]{:S(2)}) %copy-start.1) | copy-done | bytes 1048600
  3.5 1.2 %copy-done.2 = bf16[2048,256]{1,0:T(8,128)(2,1)S(1)} copy-done((bf16[2048,256]{1,0:T(8,128)(2,1)S(1)}, bf16[2048,256]{1,0:T(8,128)(2,1)}, u32[]{:S(2)}) %copy-start.2) | copy-done | bytes 1048600
  4.7 1.2 %copy-done.3 = bf16[2048,256]{1,0:T(8,128)(2,1)S(1)} copy-done((bf16[2048,256]{1,0:T(8,128)(2,1)S(1)}, bf16[2048,256]{1,0:T(8,128)(2,1)}, u32[]{:S(2)}) %copy-start.3) | copy-done | bytes 1048600
  5.9 1.2 %copy-done.4 = bf16[2048,256]{1,0:T(8,128)(2,1)S(1)} copy-done((bf16[2048,256]{1,0:T(8,128)(2,1)S(1)}, bf16[2048,256]{1,0:T(8,128)(2,1)}, u32[]{:S(2)}) %copy-start.4) | copy-done | bytes 1048600
  7.1 1.2 %copy-done.5 = bf16[256,2048]{1,0:T(8,128)(2,1)S(1)} copy-done((bf16[256,2048]{1,0:T(8,128)(2,1)S(1)}, bf16[256,2048]{1,0:T(8,128)(2,1)}, u32[]{:S(2)}) %copy-start.5) | copy-done | bytes 1048600
  8.4 0.8 %copy-done.9 = bf16[16,2048]{1,0:T(8,128)(2,1)S(1)} copy-done((bf16[16,2048]{1,0:T(8,128)(2,1)S(1)}, bf16[16,2048]{1,0:T(8,128)(2,1)}, u32[]{:S(2)}) %copy-start.9) | copy-done | bytes 65560
  9.2 0.8 %copy-done.11 = bf16[2048,8]{0,1:T(8,128)(2,1)S(1)} copy-done((bf16[2048,8]{0,1:T(8,128)(2,1)S(1)}, bf16[2048,8]{0,1:T(8,128)(2,1)}, u32[]{:S(2)}) %copy-start.11) | copy-done | bytes 32792
  10.0 0.8 %copy-done.12 = bf16[2048,8]{0,1:T(8,128)(2,1)S(1)} copy-done((bf16[2048,8]{0,1:T(8,128)(2,1)S(1)}, bf16[2048,8]{0,1:T(8,128)(2,1)}, u32[]{:S(2)}) %copy-start.12) | copy-done | bytes 32792
  10.7 0.7 %copy-done.13 = f32[2048]{0:T(1024)S(1)} copy-done((f32[2048]{0:T(1024)S(1)}, f32[2048]{0:T(1024)}, u32[]{:S(2)}) %copy-start.13) | copy-done | bytes 8216
  11.4 0.7 %copy-done.17 = f32[8]{0:T(128)S(1)} copy-done((f32[8]{0:T(128)S(1)}, f32[8]{0:T(128)}, u32[]{:S(2)}) %copy-start.17) | copy-done | bytes 56
  12.1 0.7 %copy-done.18 = f32[128]{0:T(128)S(1)} copy-done((f32[128]{0:T(128)S(1)}, f32[128]{0:T(128)}, u32[]{:S(2)}) %copy-start.18) | copy-done | bytes 536
  12.7 0.0 copy-start.14
  12.7 0.0 copy-start.15
  12.8 0.0 copy-start.16
  12.8 4.7 %mixer.1 = (f32[16,2048]{1,0:T(8,128)S(1)}, f32[16,2,128,128]{3,2,1,0:T(8,128)}) custom-call(bf16[16,2048]{1,0:T(8,128)(2,1)S(1)} %copy-done.9, f32[1,2048]{1,0:T(1,128)S(1)} %bitcast.10, bf16[8,2048]{1,0:T(8,128)(2,1)S(1)} %bitcast.8, bf16[8,2048]{1,0:T(8,128)(2,1)S(1)} %bitcast.9, f32[1,8]{1,0:T(1,128)S(1)} %bitcast.14, f32[1,128]{1,0:T(1,128)S(1)} %bitcast.15, ...), custom_call_target="tpu_custom_call" | custom-call | tf_op jit(solution)/shard_map/mixer/pallas_call | solution.py:130
  17.5 0.0 copy-done.6
  17.5 0.0 copy-done.7
  17.5 0.0 copy-done.8
  17.5 0.0 copy-done.10
  17.5 0.0 copy-done.14
  17.6 42.8 %exchange.1 = bf16[16,512]{1,0:T(8,128)(2,1)S(1)} custom-call(f32[16,2048]{1,0:T(8,128)S(1)} %get-tuple-element.4.partial_ref, bf16[16,2048]{1,0:T(8,128)(2,1)S(1)} %copy-done.10, s32[2,16]{1,0:T(2,128)S(1)} %bitcast.12, f32[2,16]{1,0:T(2,128)S(1)} %bitcast.13, f32[1,2048]{1,0:T(1,128)S(1)} %bitcast.11, bf16[1,2048,256]{2,1,0:T(8,128)(2,1)S(1)} %copy-done.6, ...), custom_call_target="tpu_custom_call" | custom-call | tf_op jit(solution)/shard_map/exchange/pallas_call | solution.py:427
  60.4 0.6 copy.21
  (17 shorter events, 0.0 us)
Async XLA Ops:
  0.6 1.6 %copy-start = (f32[16,2,128,128]{3,2,1,0:T(8,128)S(1)}, f32[16,2,128,128]{3,2,1,0:T(8,128)}, u32[]{:S(2)}) copy-start(f32[16,2,128,128]{3,2,1,0:T(8,128)} %state_hbm.1) | copy-start | bytes 6291460
  2.2 1.2 %copy-start.1 = (bf16[2048,256]{1,0:T(8,128)(2,1)S(1)}, bf16[2048,256]{1,0:T(8,128)(2,1)}, u32[]{:S(2)}) copy-start(bf16[2048,256]{1,0:T(8,128)(2,1)} %q_hbm.1) | copy-start | bytes 3145732
  3.5 1.2 %copy-start.2 = (bf16[2048,256]{1,0:T(8,128)(2,1)S(1)}, bf16[2048,256]{1,0:T(8,128)(2,1)}, u32[]{:S(2)}) copy-start(bf16[2048,256]{1,0:T(8,128)(2,1)} %k_hbm.1) | copy-start | bytes 3145732
  4.7 1.2 %copy-start.3 = (bf16[2048,256]{1,0:T(8,128)(2,1)S(1)}, bf16[2048,256]{1,0:T(8,128)(2,1)}, u32[]{:S(2)}) copy-start(bf16[2048,256]{1,0:T(8,128)(2,1)} %v_hbm.1) | copy-start | bytes 3145732
  5.9 1.2 %copy-start.4 = (bf16[2048,256]{1,0:T(8,128)(2,1)S(1)}, bf16[2048,256]{1,0:T(8,128)(2,1)}, u32[]{:S(2)}) copy-start(bf16[2048,256]{1,0:T(8,128)(2,1)} %z_hbm.1) | copy-start | bytes 3145732
  7.1 1.2 %copy-start.5 = (bf16[256,2048]{1,0:T(8,128)(2,1)S(1)}, bf16[256,2048]{1,0:T(8,128)(2,1)}, u32[]{:S(2)}) copy-start(bf16[256,2048]{1,0:T(8,128)(2,1)} %o_hbm.1) | copy-start | bytes 3145732
  8.4 0.8 %copy-start.9 = (bf16[16,2048]{1,0:T(8,128)(2,1)S(1)}, bf16[16,2048]{1,0:T(8,128)(2,1)}, u32[]{:S(2)}) copy-start(bf16[16,2048]{1,0:T(8,128)(2,1)} %tokens_ref.3) | copy-start | bytes 196612
  9.2 0.8 %copy-start.11 = (bf16[2048,8]{0,1:T(8,128)(2,1)S(1)}, bf16[2048,8]{0,1:T(8,128)(2,1)}, u32[]{:S(2)}) copy-start(bf16[2048,8]{0,1:T(8,128)(2,1)} %param.25) | copy-start | bytes 98308
  10.0 0.8 %copy-start.12 = (bf16[2048,8]{0,1:T(8,128)(2,1)S(1)}, bf16[2048,8]{0,1:T(8,128)(2,1)}, u32[]{:S(2)}) copy-start(bf16[2048,8]{0,1:T(8,128)(2,1)} %param.26) | copy-start | bytes 98308
  10.7 0.7 %copy-start.13 = (f32[2048]{0:T(1024)S(1)}, f32[2048]{0:T(1024)}, u32[]{:S(2)}) copy-start(f32[2048]{0:T(1024)} %param.20) | copy-start | bytes 24580
  11.4 0.7 %copy-start.17 = (f32[8]{0:T(128)S(1)}, f32[8]{0:T(128)}, u32[]{:S(2)}) copy-start(f32[8]{0:T(128)} %param.27) | copy-start | bytes 100
  12.1 0.7 %copy-start.18 = (f32[128]{0:T(128)S(1)}, f32[128]{0:T(128)}, u32[]{:S(2)}) copy-start(f32[128]{0:T(128)} %param.28) | copy-start | bytes 1540
  12.7 4.8 %copy-start.6 = (bf16[1,2048,256]{2,1,0:T(8,128)(2,1)S(1)}, bf16[1,2048,256]{2,1,0:T(8,128)(2,1)}, u32[]{:S(2)}) copy-start(bf16[1,2048,256]{2,1,0:T(8,128)(2,1)} %gate_hbm.1) | copy-start | bytes 3145732
  12.7 4.8 %copy-start.7 = (bf16[1,2048,256]{2,1,0:T(8,128)(2,1)S(1)}, bf16[1,2048,256]{2,1,0:T(8,128)(2,1)}, u32[]{:S(2)}) copy-start(bf16[1,2048,256]{2,1,0:T(8,128)(2,1)} %up_hbm.1) | copy-start | bytes 3145732
  12.7 4.8 %copy-start.8 = (bf16[1,256,2048]{2,1,0:T(8,128)(2,1)S(1)}, bf16[1,256,2048]{2,1,0:T(8,128)(2,1)}, u32[]{:S(2)}) copy-start(bf16[1,256,2048]{2,1,0:T(8,128)(2,1)} %down_hbm.1) | copy-start | bytes 3145732
  12.7 4.8 %copy-start.10 = (bf16[16,2048]{1,0:T(8,128)(2,1)S(1)}, bf16[16,2048]{1,0:T(8,128)(2,1)}, u32[]{:S(2)}) copy-start(bf16[16,2048]{1,0:T(8,128)(2,1)} %tokens_ref.3) | copy-start | bytes 196612
  12.7 4.8 %copy-start.14 = (f32[2048]{0:T(1024)S(1)}, f32[2048]{0:T(1024)}, u32[]{:S(2)}) copy-start(f32[2048]{0:T(1024)} %param.30) | copy-start | bytes 24580
  12.7 4.8 %copy-start.15 = (s32[16,2]{0,1:T(2,128)S(1)}, s32[16,2]{0,1:T(2,128)}, u32[]{:S(2)}) copy-start(s32[16,2]{0,1:T(2,128)} %param.31) | copy-start | bytes 388
  12.8 4.8 %copy-start.16 = (f32[16,2]{0,1:T(2,128)S(1)}, f32[16,2]{0,1:T(2,128)}, u32[]{:S(2)}) copy-start(f32[16,2]{0,1:T(2,128)} %param.32) | copy-start | bytes 388

commit v3 on v2

v3 whole, which is shorter than its diff:
```python
import functools

import jax
import jax.numpy as jnp
from jax import lax
from jax.experimental import pallas as pl
from jax.experimental.pallas import tpu as pltpu
from jax.sharding import PartitionSpec as P

EPS = 1e-06
MESH = pl.DeviceIdType.MESH
F32 = jnp.float32
BF16 = jnp.bfloat16
HIGHEST = lax.Precision.HIGHEST
CORES = 2
RING_Y = 4
CAP = 4
PARTS = 4
LANE = 128
TILE = CAP * PARTS
GROUPS = 8
CHUNKS = ((0, 16), (16, 32))
PIECES = (((0, 16),), ((24, 32), (16, 24)))
STATE_CHUNKS = 4
VMEM_GRANT = 63 * 1024 * 1024
EXCHANGE_GRANT = 53 * 1024 * 1024


def rms_scale(values, gain):
    return values * lax.rsqrt(jnp.mean(values * values, axis=-1, keepdims=True) + EPS) * gain


def unit_rows(values):
    return values * lax.rsqrt(jnp.sum(values * values, axis=-1, keepdims=True) + EPS)


def hop(slot, ring_z):
    i, dy = slot // RING_Y, slot % RING_Y
    dz = (i % 2) * ((i + 1) // 2) + (1 - i % 2) * ((ring_z - i // 2) % ring_z)
    return dz, dy


def iota(shape, dim):
    return lax.broadcasted_iota(jnp.int32, shape, dim)


def fetch(pairs, sems):
    copies = [pltpu.make_async_copy(src, dst, sems.at[i]) for i, (src, dst) in enumerate(pairs)]
    for copy in copies:
        copy.start()
    return copies


def heads_of(proj):
    proj = proj.astype(BF16).astype(F32)
    return [jax.nn.silu(proj[:, at : at + LANE]) for at in range(0, proj.shape[1], LANE)]


def mixer_kernel(
    heads, tokens_hbm, gain_hbm, beta_hbm, decay_hbm, rate_hbm, k_hbm, q_hbm, v_hbm, state_hbm,
    read_hbm, new_hbm, tokens, gain, beta, decay, rate, wk, wq, wv, state, read, small_sem, load_sem, state_sem, out_sem,
    read_sem,
):
    tp = lax.axis_index("tp")
    seqs = tokens.shape[0]
    step = seqs // STATE_CHUNKS

    small = fetch(
        ((tokens_hbm, tokens), (gain_hbm, gain), (beta_hbm, beta), (decay_hbm, decay), (rate_hbm, rate)), small_sem
    )
    loads = fetch(((k_hbm, wk), (q_hbm, wq), (v_hbm, wv)), load_sem)
    parts = [pl.ds(c * step, step) for c in range(STATE_CHUNKS)]

    for copy in small + loads:
        copy.wait()
    reads = fetch([(state_hbm.at[part], state.at[part]) for part in parts], state_sem)
    normed = rms_scale(tokens[...].astype(F32), gain[...]).astype(BF16)

    def project(weight):
        return heads_of(jnp.dot(normed, weight[...], preferred_element_type=F32))

    keys = [unit_rows(k) for k in project(wk)]
    queries = [unit_rows(q) * LANE ** (-0.5) for q in project(wq)]
    values = project(wv)
    filler = [jnp.zeros((LANE - 2 * heads * seqs, LANE), F32)]
    columns = jnp.concatenate(keys + queries + filler, axis=0).T

    def by_head(weight):
        return lax.dot_general(normed, weight[...], (((1,), (1,)), ((), ())), preferred_element_type=F32)

    strength = jax.nn.sigmoid(by_head(beta))
    fading = jnp.exp(-rate[...] * jax.nn.softplus(by_head(decay)))

    def own_head(values, h):
        chosen = iota(values.shape, 1) == tp * heads + h
        column = jnp.sum(jnp.where(chosen, values, 0.0), axis=1, keepdims=True)
        return jnp.broadcast_to(column, (seqs, LANE))

    strengths = [own_head(strength, h) for h in range(heads)]
    fadings = [own_head(fading, h) for h in range(heads)]

    writes = []
    for c, part in enumerate(parts):
        reads[c].wait()
        for t in range(c * step, (c + 1) * step):
            for h in range(heads):
                j = h * seqs + t
                key, query = columns[:, j : j + 1], columns[:, heads * seqs + j : heads * seqs + j + 1]
                fade = fadings[h][t : t + 1]
                old = state[t, h]
                recall = jnp.sum(old * key, axis=0, keepdims=True)
                delta = strengths[h][t : t + 1] * (values[h][t : t + 1] - fade * recall)
                new = fade * old + key * delta
                state[t, h] = new
                read[t : t + 1, h * LANE : (h + 1) * LANE] = jnp.sum(new * query, axis=0, keepdims=True)
        write = pltpu.make_async_copy(state.at[part], new_hbm.at[part], out_sem.at[c])
        write.start()
        writes.append(write)
    write = pltpu.make_async_copy(read, read_hbm.at[0:seqs], read_sem)
    write.start()
    write.wait()
    for write in writes:
        write.wait()


def mixer(
    tokens, recur_state, attn_gain, query_weight, key_weight, value_weight, beta_weight, decay_weight, decay_rate
):
    seqs, model = tokens.shape
    heads, size = recur_state.shape[1:3]
    anywhere = pl.BlockSpec(memory_space=pltpu.HBM)
    dma = pltpu.SemaphoreType.DMA
    small = (tokens, attn_gain.reshape(1, -1), beta_weight.T, decay_weight.T, decay_rate.reshape(1, -1))
    return pl.pallas_call(
        functools.partial(mixer_kernel, heads),
        name="mixer",
        out_shape=(
            jax.ShapeDtypeStruct((model, heads * size), F32),
            jax.ShapeDtypeStruct(recur_state.shape, F32),
        ),
        in_specs=[anywhere] * 9,
        out_specs=(anywhere, anywhere),
        scratch_shapes=[pltpu.VMEM(array.shape, array.dtype) for array in small]
        + [pltpu.VMEM((model, heads * size), BF16)] * 3
        + [
            pltpu.VMEM(recur_state.shape, F32),
            pltpu.VMEM((seqs, heads * size), F32),
            dma((5,)),
            dma((3,)),
            dma((STATE_CHUNKS,)),
            dma((STATE_CHUNKS,)),
            dma,
        ],
        compiler_params=pltpu.CompilerParams(vmem_limit_bytes=VMEM_GRANT),
    )(*small, key_weight, query_weight, value_weight, recur_state)


def exchange_kernel(
    lanes, groups, tokens, attn_gain, head_gain, ffn_gain, routes_flat, rw_flat,
    read_hbm, z_hbm, o_hbm, gate_hbm, up_hbm, down_hbm, out_ref,
    read, wz, wo,
    partial, branch, packed, rows, wide_in, wdown, ysend, yrecv, gathered, back,
    ready, head_sem, local_sem, swap_send, swap_recv, b_send, b_recv, c_send, c_recv, d_send, d_recv,
    f_send, f_recv, g_send, g_recv,
):
    ring_z = groups // (RING_Y * CORES)
    plane = ring_z * RING_Y
    per_group = plane // GROUPS
    tp = lax.axis_index("tp")
    ep = lax.axis_index("ep")
    core = ep % CORES
    y = (ep // CORES) % RING_Y
    z = ep // (CORES * RING_Y)
    seqs, width = tokens.shape[0], tokens.shape[1] // lanes

    zs = [(z + dz) % ring_z for dz in range(ring_z)]
    ys = [(y + dy) % RING_Y for dy in range(RING_Y)]
    z_part = [zz * (RING_Y * CORES) for zz in zs]
    y_part = [yy * CORES + core for yy in ys]

    def forward(slot):
        dz, dy = hop(slot, ring_z)
        return z_part[dz] + y_part[dy]

    def backward(slot):
        dz, dy = hop(slot, ring_z)
        return z_part[-dz % ring_z] + y_part[-dy % RING_Y]

    partner = ep + 1 - 2 * core
    nearest_last = list(range(plane - 1, 0, -1))

    z_in, read_in, o_in = fetch(((z_hbm, wz), (read_hbm.at[0:seqs], read), (o_hbm, wo)), head_sem)

    barrier = pltpu.get_barrier_semaphore()
    for slot in nearest_last:
        pl.semaphore_signal(barrier, inc=1, device_id=(forward(slot), tp), device_id_type=MESH)
    for dx in range(1, lanes):
        pl.semaphore_signal(barrier, inc=1, device_id=(ep, (tp + dx) % lanes), device_id_type=MESH)

    @pl.when(core == 0)
    def _():
        pl.semaphore_signal(barrier, inc=1, device_id=(partner, tp), device_id_type=MESH)

    hidden = gate_hbm.shape[2]

    def weights(s):
        return (
            (gate_hbm.at[0], wide_in.at[s, :, 0:hidden]),
            (up_hbm.at[0], wide_in.at[s, :, hidden : 2 * hidden]),
            (down_hbm.at[0], wdown.at[s * hidden : (s + 1) * hidden, :]),
        )

    loads = fetch(weights(0), local_sem)

    normed = rms_scale(tokens[...].astype(F32), attn_gain[...]).astype(BF16)
    z_in.wait()
    read_in.wait()
    gates = heads_of(jnp.dot(normed, wz[...], preferred_element_type=F32))
    headed = [
        (rms_scale(read[:, h * LANE : (h + 1) * LANE], head_gain[...]) * gate).astype(BF16) for h, gate in enumerate(gates)
    ]
    o_in.wait()
    shares = jnp.dot(jnp.concatenate(headed, axis=1), wo[...], preferred_element_type=F32)
    partial[...] = shares.astype(BF16)

    pl.semaphore_wait(barrier, plane - 1 + lanes - 1 + core)

    sums = []
    for dx in range(1, lanes):
        to = (tp + dx) % lanes
        copy = pltpu.make_async_remote_copy(
            src_ref=partial.at[:, pl.ds(pl.multiple_of(to * width, LANE), width)],
            dst_ref=branch.at[dx - 1],
            send_sem=b_send.at[dx - 1],
            recv_sem=b_recv.at[dx - 1],
            device_id=(ep, to),
            device_id_type=MESH,
        )
        copy.start()
        sums.append(copy)

    swaps = [
        pltpu.make_async_remote_copy(
            src_ref=src, dst_ref=dst, send_sem=swap_send.at[i], recv_sem=swap_recv.at[i],
            device_id=(partner, tp), device_id_type=MESH,
        )
        for i, (src, dst) in enumerate(weights(1))
    ]

    @pl.when(core == 1)
    def _():
        pl.semaphore_signal(ready, inc=1, device_id=(partner, tp), device_id_type=MESH)
        for swap in swaps:
            swap.start()

    experts = groups // 4
    eye = (iota((seqs, seqs), 0) == iota((seqs, seqs), 1)).astype(F32)

    def upright(flat):
        return lax.dot_general(eye, flat, (((1,), (1,)), ((), ())), preferred_element_type=F32, precision=HIGHEST)

    routes = upright(routes_flat[...].astype(F32)).astype(jnp.int32)
    rw = upright(rw_flat[...])
    onehots = [(routes[:, k : k + 1] == iota((seqs, experts), 1)).astype(F32) for k in range(routes.shape[1])]
    earlier = (iota((seqs, seqs), 1) < iota((seqs, seqs), 0)).astype(F32)
    counts = jnp.dot(earlier, sum(onehots), preferred_element_type=F32)
    targets = []
    for k, onehot in enumerate(onehots):
        position = jnp.sum(counts * onehot, axis=1, keepdims=True).astype(jnp.int32)
        targets.append(routes[:, k : k + 1] * CAP + position)
    tall = [jnp.concatenate([t] * PARTS, axis=0) for t in targets]
    tall_w = [jnp.concatenate([rw[:, k : k + 1]] * PARTS, axis=0) for k in range(len(targets))]
    height = PARTS * seqs
    lane_id = iota((height, experts * TILE), 1)
    slot_of = (lane_id // TILE) * CAP + lane_id % CAP
    same_part = (lane_id % TILE) // CAP == iota((height, experts * TILE), 0) // seqs
    chosen = (tall[0] == slot_of) | (tall[1] == slot_of)
    select = (chosen & same_part).astype(F32).astype(BF16)

    mine = pl.ds(pl.multiple_of(tp * width, LANE), width)
    total = partial[:, mine].astype(F32)
    for dx, copy in enumerate(sums):
        copy.wait_recv()
        total = total + branch[dx].astype(F32)
    resid = (tokens[:, mine].astype(F32) + total.astype(BF16).astype(F32)).astype(BF16)
    stacked = jnp.concatenate([resid[:, q * LANE : (q + 1) * LANE] for q in range(PARTS)], axis=0)
    picked = lax.dot_general(select, stacked, (((0,), (0,)), ((), ())), preferred_element_type=F32)
    packed[...] = picked.astype(BF16)

    z_rows = [zz * (RING_Y // 2 * TILE) for zz in zs]
    y_rows = [yy // 2 * TILE for yy in ys]
    for slot in range(1, plane):
        dz, dy = hop(slot, ring_z)
        pltpu.make_async_remote_copy(
            src_ref=packed.at[pl.ds(pl.multiple_of(z_rows[dz] + y_rows[dy], TILE), TILE), :],
            dst_ref=rows.at[tp, slot * TILE : (slot + 1) * TILE, :],
            send_sem=c_send,
            recv_sem=c_recv.at[slot // per_group],
            device_id=(forward(slot), tp),
            device_id_type=MESH,
        ).start()

    rows[tp, 0:TILE, :] = packed[pl.ds(pl.multiple_of(z_rows[0] + y_rows[0], TILE), TILE), :]

    @pl.when(core == 0)
    def _():
        pl.semaphore_wait(ready, 1)
        for swap in swaps:
            swap.start()

    def landed(ref, send_sem, recv_sem):
        return pltpu.make_async_remote_copy(
            src_ref=ref, dst_ref=ref, send_sem=send_sem, recv_sem=recv_sem, device_id=(partner, tp), device_id_type=MESH
        )

    def shuffle(slots):
        high = slots * CAP
        shape = (slots * TILE, slots * TILE)

        def hit(dim):
            index = iota(shape, dim)
            part = sum((index >= q * high).astype(jnp.int32) for q in range(1, PARTS))
            rest = index - part * high
            return ((rest // CAP) * TILE + part * CAP + rest % CAP == iota(shape, 1 - dim)).astype(F32).astype(BF16)

        return hit(0), hit(1)

    shuffles = [shuffle(last - first) for first, last in CHUNKS]

    spreads = [[] for _ in CHUNKS]
    for g in range(GROUPS):
        first, last = g * per_group * TILE, (g + 1) * per_group * TILE
        fresh = max(first, TILE)
        landed(rows.at[tp, fresh:last, :], c_send, c_recv.at[g]).wait_recv()
        for dx in range(1, lanes):
            copy = pltpu.make_async_remote_copy(
                src_ref=rows.at[tp, first:last, :],
                dst_ref=rows.at[tp, first:last, :],
                send_sem=d_send.at[g, dx - 1],
                recv_sem=d_recv.at[g, dx - 1],
                device_id=(ep, (tp + dx) % lanes),
                device_id_type=MESH,
            )
            copy.start()
            chunk = [low <= g * per_group < top for low, top in CHUNKS].index(True)
            spreads[chunk].append((g, dx, first, last, copy))

    lane_id = iota((height, plane * TILE), 1)
    dz, dy = hop(lane_id // TILE, ring_z)
    expert = ((z + dz) % ring_z) * (RING_Y // 2) + ((y + dy) % RING_Y) // 2
    slot_of = expert * CAP + lane_id % CAP
    same_part = (lane_id % TILE) // CAP == iota((height, plane * TILE), 0) // seqs
    combine = jnp.zeros((height, plane * TILE), F32)
    for target, weight in zip(tall, tall_w):
        combine = combine + jnp.where((target == slot_of) & same_part, weight, 0.0)

    gives = []
    for c, (low, top) in enumerate(CHUNKS):
        here = slice(low * TILE, top * TILE)
        high = (top - low) * CAP
        sort, unsort = shuffles[c]
        for g, dx, first, last, copy in spreads[c]:
            source = (tp + lanes - dx) % lanes
            landed(rows.at[source, first:last, :], d_send.at[g, dx - 1], d_recv.at[g, dx - 1]).wait_recv()
        wide = jnp.concatenate([rows[x, here, :] for x in range(lanes)], axis=1)
        ordered = jnp.dot(sort, wide, preferred_element_type=F32)
        arrived = jnp.concatenate(
            [ordered[q * high : (q + 1) * high, x * LANE : (x + 1) * LANE] for x in range(lanes) for q in range(PARTS)],
            axis=1,
        )
        ffn_in = rms_scale(arrived, ffn_gain[...]).astype(BF16)
        if c == 0:
            for load in loads:
                load.wait()
            for swap in swaps:
                swap.wait_recv()
        units = []
        for s in range(CORES):
            both = jnp.dot(ffn_in, wide_in[s], preferred_element_type=F32)
            units.append((jax.nn.silu(both[:, :hidden]) * both[:, hidden:]).astype(BF16))
        part = jnp.dot(jnp.concatenate(units, axis=1), wdown[...], preferred_element_type=F32).astype(BF16)
        tall_part = jnp.concatenate(
            [
                jnp.concatenate([part[:, (x * PARTS + q) * LANE : (x * PARTS + q + 1) * LANE] for x in range(lanes)], axis=1)
                for q in range(PARTS)
            ],
            axis=0,
        )
        split = jnp.dot(unsort, tall_part, preferred_element_type=F32).astype(BF16)
        for x in range(lanes):
            ysend[x, here, :] = split[:, x * LANE : (x + 1) * LANE]
        for first, last in PIECES[c]:
            piece = slice(first * TILE, last * TILE)
            copies = []
            for dx in range(1, lanes):
                to = (tp + dx) % lanes
                copy = pltpu.make_async_remote_copy(
                    src_ref=ysend.at[to, piece, :],
                    dst_ref=yrecv.at[dx - 1, piece, :],
                    send_sem=f_send.at[len(gives), dx - 1],
                    recv_sem=f_recv.at[len(gives), dx - 1],
                    device_id=(ep, to),
                    device_id_type=MESH,
                )
                copy.start()
                copies.append(copy)
            gives.append((first, last, copies))

    for first, last, copies in gives:
        piece = slice(first * TILE, last * TILE)
        own = ysend[tp, piece, :].astype(F32)
        for dx, copy in enumerate(copies):
            copy.wait_recv()
            own = own + yrecv[dx, piece, :].astype(F32)
        gathered[piece, :] = own.astype(BF16)
        for slot in range(last - 1, max(1, first) - 1, -1):
            pltpu.make_async_remote_copy(
                src_ref=gathered.at[slot * TILE : (slot + 1) * TILE, :],
                dst_ref=back.at[slot * TILE : (slot + 1) * TILE, :],
                send_sem=g_send,
                recv_sem=g_recv,
                device_id=(backward(slot), tp),
                device_id_type=MESH,
            ).start()
        if first == 0:
            back[0:TILE, :] = gathered[0:TILE, :]

    for copy in sums:
        copy.wait_send()
    for swap in swaps:
        swap.wait_send()
    landed(gathered.at[TILE : plane * TILE, :], c_send, g_recv).wait_send()
    for copies in spreads:
        for _, _, _, _, copy in copies:
            copy.wait_send()
    for _, _, copies in gives:
        for copy in copies:
            copy.wait_send()
    landed(gathered.at[TILE : plane * TILE, :], g_send, g_recv).wait_send()

    landed(back.at[TILE : plane * TILE, :], g_send, g_recv).wait_recv()
    moe = jnp.dot(combine, back[...].astype(F32), preferred_element_type=F32, precision=HIGHEST)
    moe = jnp.concatenate([moe[q * seqs : (q + 1) * seqs] for q in range(PARTS)], axis=1)
    out_ref[...] = (resid.astype(F32) + moe).astype(BF16)


def exchange(
    readout, tokens, attn_gain, head_gain, ffn_gain, routes, route_weight, outgate_weight, output_weight, expert_gate,
    expert_up, expert_down,
):
    lanes, groups = lax.axis_size("tp"), lax.axis_size("ep")
    seqs, model = tokens.shape
    width = model // lanes
    plane = groups // CORES
    hidden = expert_gate.shape[2]
    anywhere = pl.BlockSpec(memory_space=pltpu.HBM)
    dma = pltpu.SemaphoreType.DMA
    small = (
        tokens, attn_gain.reshape(1, -1), head_gain.reshape(1, -1), ffn_gain.reshape(1, -1), routes.T, route_weight.T
    )
    weights = (outgate_weight, output_weight)
    vmem = pl.BlockSpec(memory_space=pltpu.VMEM)
    return pl.pallas_call(
        functools.partial(exchange_kernel, lanes, groups),
        name="exchange",
        out_shape=jax.ShapeDtypeStruct((seqs, width), BF16),
        in_specs=[vmem] * len(small) + [anywhere] * 6,
        out_specs=vmem,
        scratch_shapes=[pltpu.VMEM((seqs, readout.shape[1]), F32)]
        + [pltpu.VMEM(array.shape, array.dtype) for array in weights]
        + [
            pltpu.VMEM((seqs, model), BF16),
            pltpu.VMEM((lanes - 1, seqs, width), BF16),
            pltpu.VMEM((groups // 4 * TILE, LANE), BF16),
            pltpu.VMEM((lanes, plane * TILE, LANE), BF16),
            pltpu.VMEM((CORES, model, 2 * hidden), BF16),
            pltpu.VMEM((CORES * hidden, model), BF16),
            pltpu.VMEM((lanes, plane * TILE, LANE), BF16),
            pltpu.VMEM((lanes - 1, plane * TILE, LANE), BF16),
            pltpu.VMEM((plane * TILE, LANE), BF16),
            pltpu.VMEM((plane * TILE, LANE), BF16),
            pltpu.SemaphoreType.REGULAR,
            dma((3,)),
            dma((3,)),
            dma((3,)),
            dma((3,)),
            dma((lanes - 1,)),
            dma((lanes - 1,)),
            dma,
            dma((GROUPS,)),
            dma((GROUPS, lanes - 1)),
            dma((GROUPS, lanes - 1)),
            dma((sum(map(len, PIECES)), lanes - 1)),
            dma((sum(map(len, PIECES)), lanes - 1)),
            dma,
            dma,
        ],
        compiler_params=pltpu.CompilerParams(collective_id=0, has_side_effects=True, vmem_limit_bytes=EXCHANGE_GRANT),
    )(*small, readout, *weights, expert_gate, expert_up, expert_down)


def local(
    tokens,
    recur_state,
    attn_gain,
    query_weight,
    key_weight,
    value_weight,
    outgate_weight,
    beta_weight,
    decay_weight,
    decay_rate,
    head_gain,
    output_weight,
    ffn_gain,
    routes,
    route_weight,
    expert_gate,
    expert_up,
    expert_down,
):
    readout, new_state = mixer(
        tokens, recur_state, attn_gain, query_weight, key_weight, value_weight, beta_weight, decay_weight, decay_rate
    )
    mixed = exchange(
        readout, tokens, attn_gain, head_gain, ffn_gain, routes, route_weight, outgate_weight, output_weight, expert_gate,
        expert_up, expert_down,
    )
    return (mixed, new_state)


def solution(mesh):
    return jax.shard_map(
        local,
        mesh=mesh,
        in_specs=(
            P("ep", None),
            P("ep", "tp", None, None),
            P(),
            P(None, "tp"),
            P(None, "tp"),
            P(None, "tp"),
            P(None, "tp"),
            P(),
            P(),
            P(),
            P(),
            P("tp", None),
            P(),
            P("ep", None),
            P("ep", None),
            P("ep", None, "tp"),
            P("ep", None, "tp"),
            P("ep", "tp", None),
        ),
        out_specs=(P("ep", "tp"), P("ep", "tp", None, None)),
        check_vma=False,
    )
```

time: 61.5 us -> 45.3 us (0.74)
  local copies, waits for them, and re-layouts: 12.7 us -> 0.63 us
  Pallas kernels: 47.5 us -> 43.8 us
    unnamed x39 -> x13, local copies, waits for them, and re-layouts: 12.7 us -> 0.63 us
    pallas_call x1, Pallas kernels: 42.8 us -> 38.3 us  [exchange(): pl.pallas_call(functools.partial(exchange_kernel, lanes, groups), name='e...]
    pallas_call x1, Pallas kernels: 4.73 us -> 5.47 us  [mixer(): pl.pallas_call(functools.partial(mixer_kernel, heads), name='mixer', out_...]
where the time goes in v3:
time: 45.3 us; the launch traced here: 45.2 us
  Pallas kernels  43.8 us (97%)
  between operations  0.75 us (2%)
  local copies, waits for them, and re-layouts  0.63 us (1%)
    pallas_call x1, Pallas kernels, exchange(): pl.pallas_call(functools.partial(exchange_kernel, lanes, groups), name='e...  38.3 us
    pallas_call x1, Pallas kernels, mixer(): pl.pallas_call(functools.partial(mixer_kernel, heads), name='mixer', out_...  5.47 us

profile of v3, /device:TPU:32, one launch (start us, length us, event | category | flops | bytes accessed | tf_op | source)
XLA Modules:
  0.0 45.2 jit_solution(8161834514581665182)
XLA Ops:
  0.6 0.0 copy-start
  0.6 0.0 copy-start.1
  0.7 0.0 copy-start.2
  0.7 0.0 copy-start.3
  0.7 0.0 copy-start.4
  0.7 0.0 copy-start.5
  0.7 5.5 %mixer.1 = (f32[2048,256]{1,0:T(8,128)}, f32[16,2,128,128]{3,2,1,0:T(8,128)}) custom-call(bf16[16,2048]{1,0:T(8,128)(2,1)} %tokens.1, f32[1,2048]{1,0:T(1,128)} %bitcast.8, bf16[8,2048]{1,0:T(8,128)(2,1)} %bitcast.14, bf16[8,2048]{1,0:T(8,128)(2,1)} %bitcast.15, f32[1,8]{1,0:T(1,128)} %bitcast.16, bf16[2048,256]{1,0:T(8,128)(2,1)} %k_hbm.1, ...), custom_call_target="tpu_custom_call" | custom-call | tf_op jit(solution)/shard_map/mixer/pallas_call | solution.py:134
  6.2 0.0 copy-done
  6.2 0.0 copy-done.1
  6.2 0.0 copy-done.2
  6.2 0.0 copy-done.3
  6.2 0.0 copy-done.4
  6.2 0.0 copy-done.5
  6.2 38.3 %exchange.1 = bf16[16,512]{1,0:T(8,128)(2,1)S(1)} custom-call(bf16[16,2048]{1,0:T(8,128)(2,1)S(1)} %copy-done, f32[1,2048]{1,0:T(1,128)S(1)} %bitcast.9, f32[1,128]{1,0:T(1,128)S(1)} %bitcast.13, f32[1,2048]{1,0:T(1,128)S(1)} %bitcast.10, s32[2,16]{1,0:T(2,128)S(1)} %bitcast.11, f32[2,16]{1,0:T(2,128)S(1)} %bitcast.12, ...), custom_call_target="tpu_custom_call" | custom-call | tf_op jit(solution)/shard_map/exchange/pallas_call | solution.py:463
  44.6 0.6 %copy.21 = bf16[16,512]{1,0:T(8,128)(2,1)} copy(bf16[16,512]{1,0:T(8,128)(2,1)S(1)} %exchange.1) | data formatting | bytes 32768
Async XLA Ops:
  0.6 5.5 %copy-start = (bf16[16,2048]{1,0:T(8,128)(2,1)S(1)}, bf16[16,2048]{1,0:T(8,128)(2,1)}, u32[]{:S(2)}) copy-start(bf16[16,2048]{1,0:T(8,128)(2,1)} %tokens.1) | copy-start | bytes 196612
  0.6 5.5 %copy-start.1 = (f32[2048]{0:T(1024)S(1)}, f32[2048]{0:T(1024)}, u32[]{:S(2)}) copy-start(f32[2048]{0:T(1024)} %param.20) | copy-start | bytes 24580
  0.7 5.5 %copy-start.2 = (f32[2048]{0:T(1024)S(1)}, f32[2048]{0:T(1024)}, u32[]{:S(2)}) copy-start(f32[2048]{0:T(1024)} %param.30) | copy-start | bytes 24580
  0.7 5.5 %copy-start.3 = (s32[16,2]{0,1:T(2,128)S(1)}, s32[16,2]{0,1:T(2,128)}, u32[]{:S(2)}) copy-start(s32[16,2]{0,1:T(2,128)} %param.31) | copy-start | bytes 388
  0.7 5.5 %copy-start.4 = (f32[16,2]{0,1:T(2,128)S(1)}, f32[16,2]{0,1:T(2,128)}, u32[]{:S(2)}) copy-start(f32[16,2]{0,1:T(2,128)} %param.32) | copy-start | bytes 388
  0.7 5.5 %copy-start.5 = (f32[128]{0:T(128)S(1)}, f32[128]{0:T(128)}, u32[]{:S(2)}) copy-start(f32[128]{0:T(128)} %param.28) | copy-start | bytes 1540

commit v4 on v3

--- a/solution.py
+++ b/solution.py
@@ -187,6 +187,7 @@
         return z_part[-dz % ring_z] + y_part[-dy % RING_Y]
 
     partner = ep + 1 - 2 * core
+    far_first = sorted(range(1, lanes), key=lambda dx: -min(dx, lanes - dx))
     nearest_last = list(range(plane - 1, 0, -1))
 
     z_in, read_in, o_in = fetch(((z_hbm, wz), (read_hbm.at[0:seqs], read), (o_hbm, wo)), head_sem)
@@ -226,7 +227,7 @@
     pl.semaphore_wait(barrier, plane - 1 + lanes - 1 + core)
 
     sums = []
-    for dx in range(1, lanes):
+    for dx in far_first:
         to = (tp + dx) % lanes
         copy = pltpu.make_async_remote_copy(
             src_ref=partial.at[:, pl.ds(pl.multiple_of(to * width, LANE), width)],
@@ -237,7 +238,7 @@
             device_id_type=MESH,
         )
         copy.start()
-        sums.append(copy)
+        sums.append((dx, copy))
 
     swaps = [
         pltpu.make_async_remote_copy(
@@ -279,9 +280,9 @@
 
     mine = pl.ds(pl.multiple_of(tp * width, LANE), width)
     total = partial[:, mine].astype(F32)
-    for dx, copy in enumerate(sums):
+    for dx, copy in sums:
         copy.wait_recv()
-        total = total + branch[dx].astype(F32)
+        total = total + branch[dx - 1].astype(F32)
     resid = (tokens[:, mine].astype(F32) + total.astype(BF16).astype(F32)).astype(BF16)
     stacked = jnp.concatenate([resid[:, q * LANE : (q + 1) * LANE] for q in range(PARTS)], axis=0)
     picked = lax.dot_general(select, stacked, (((0,), (0,)), ((), ())), preferred_element_type=F32)
@@ -332,7 +333,7 @@
         first, last = g * per_group * TILE, (g + 1) * per_group * TILE
         fresh = max(first, TILE)
         landed(rows.at[tp, fresh:last, :], c_send, c_recv.at[g]).wait_recv()
-        for dx in range(1, lanes):
+        for dx in far_first:
             copy = pltpu.make_async_remote_copy(
                 src_ref=rows.at[tp, first:last, :],
                 dst_ref=rows.at[tp, first:last, :],
@@ -353,6 +354,11 @@
     combine = jnp.zeros((height, plane * TILE), F32)
     for target, weight in zip(tall, tall_w):
         combine = combine + jnp.where((target == slot_of) & same_part, weight, 0.0)
+    thirds = []
+    for _ in range(3):
+        thirds.append(combine.astype(BF16))
+        combine = combine - thirds[-1].astype(F32)
+    combine = jnp.concatenate(thirds, axis=0)
 
     gives = []
     for c, (low, top) in enumerate(CHUNKS):
@@ -392,7 +398,7 @@
         for first, last in PIECES[c]:
             piece = slice(first * TILE, last * TILE)
             copies = []
-            for dx in range(1, lanes):
+            for dx in far_first:
                 to = (tp + dx) % lanes
                 copy = pltpu.make_async_remote_copy(
                     src_ref=ysend.at[to, piece, :],
@@ -403,15 +409,15 @@
                     device_id_type=MESH,
                 )
                 copy.start()
-                copies.append(copy)
+                copies.append((dx, copy))
             gives.append((first, last, copies))
 
     for first, last, copies in gives:
         piece = slice(first * TILE, last * TILE)
         own = ysend[tp, piece, :].astype(F32)
-        for dx, copy in enumerate(copies):
+        for dx, copy in sorted(copies, key=lambda pair: pair[0]):
             copy.wait_recv()
-            own = own + yrecv[dx, piece, :].astype(F32)
+            own = own + yrecv[dx - 1, piece, :].astype(F32)
         gathered[piece, :] = own.astype(BF16)
         for slot in range(last - 1, max(1, first) - 1, -1):
             pltpu.make_async_remote_copy(
@@ -425,7 +431,7 @@
         if first == 0:
             back[0:TILE, :] = gathered[0:TILE, :]
 
-    for copy in sums:
+    for _, copy in sums:
         copy.wait_send()
     for swap in swaps:
         swap.wait_send()
@@ -434,12 +440,13 @@
         for _, _, _, _, copy in copies:
             copy.wait_send()
     for _, _, copies in gives:
-        for copy in copies:
+        for _, copy in copies:
             copy.wait_send()
     landed(gathered.at[TILE : plane * TILE, :], g_send, g_recv).wait_send()
 
     landed(back.at[TILE : plane * TILE, :], g_send, g_recv).wait_recv()
-    moe = jnp.dot(combine, back[...].astype(F32), preferred_element_type=F32, precision=HIGHEST)
+    thirds = jnp.dot(combine, back[...], preferred_element_type=F32)
+    moe = thirds[:height] + thirds[height : 2 * height] + thirds[2 * height :]
     moe = jnp.concatenate([moe[q * seqs : (q + 1) * seqs] for q in range(PARTS)], axis=1)
     out_ref[...] = (resid.astype(F32) + moe).astype(BF16)
 

time: 45.3 us -> 45 us (level)
  no operation moved by 1% of the time
where the time goes in v4:
time: 45 us; the launch traced here: 44.9 us
  Pallas kernels  43.5 us (97%)
  between operations  0.75 us (2%)
  local copies, waits for them, and re-layouts  0.63 us (1%)
    pallas_call x1, Pallas kernels, exchange(): pl.pallas_call(functools.partial(exchange_kernel, lanes, groups), name='e...  38 us
    pallas_call x1, Pallas kernels, mixer(): pl.pallas_call(functools.partial(mixer_kernel, heads), name='mixer', out_...  5.47 us

profile of v4, /device:TPU:32, one launch (start us, length us, event | category | flops | bytes accessed | tf_op | source)
XLA Modules:
  0.0 44.9 jit_solution(5133766740849141336)
XLA Ops:
  0.6 0.0 copy-start
  0.6 0.0 copy-start.1
  0.7 0.0 copy-start.2
  0.7 0.0 copy-start.3
  0.7 0.0 copy-start.4
  0.7 0.0 copy-start.5
  0.7 5.5 %mixer.1 = (f32[2048,256]{1,0:T(8,128)}, f32[16,2,128,128]{3,2,1,0:T(8,128)}) custom-call(bf16[16,2048]{1,0:T(8,128)(2,1)} %tokens.1, f32[1,2048]{1,0:T(1,128)} %bitcast.8, bf16[8,2048]{1,0:T(8,128)(2,1)} %bitcast.14, bf16[8,2048]{1,0:T(8,128)(2,1)} %bitcast.15, f32[1,8]{1,0:T(1,128)} %bitcast.16, bf16[2048,256]{1,0:T(8,128)(2,1)} %k_hbm.1, ...), custom_call_target="tpu_custom_call" | custom-call | tf_op jit(solution)/shard_map/mixer/pallas_call | solution.py:134
  6.2 0.0 copy-done
  6.2 0.0 copy-done.1
  6.2 0.0 copy-done.2
  6.2 0.0 copy-done.3
  6.2 0.0 copy-done.4
  6.2 0.0 copy-done.5
  6.2 38.0 %exchange.1 = bf16[16,512]{1,0:T(8,128)(2,1)S(1)} custom-call(bf16[16,2048]{1,0:T(8,128)(2,1)S(1)} %copy-done, f32[1,2048]{1,0:T(1,128)S(1)} %bitcast.9, f32[1,128]{1,0:T(1,128)S(1)} %bitcast.13, f32[1,2048]{1,0:T(1,128)S(1)} %bitcast.10, s32[2,16]{1,0:T(2,128)S(1)} %bitcast.11, f32[2,16]{1,0:T(2,128)S(1)} %bitcast.12, ...), custom_call_target="tpu_custom_call" | custom-call | tf_op jit(solution)/shard_map/exchange/pallas_call | solution.py:470
  44.3 0.6 %copy.21 = bf16[16,512]{1,0:T(8,128)(2,1)} copy(bf16[16,512]{1,0:T(8,128)(2,1)S(1)} %exchange.1) | data formatting | bytes 32768
Async XLA Ops:
  0.6 5.5 %copy-start = (bf16[16,2048]{1,0:T(8,128)(2,1)S(1)}, bf16[16,2048]{1,0:T(8,128)(2,1)}, u32[]{:S(2)}) copy-start(bf16[16,2048]{1,0:T(8,128)(2,1)} %tokens.1) | copy-start | bytes 196612
  0.6 5.5 %copy-start.1 = (f32[2048]{0:T(1024)S(1)}, f32[2048]{0:T(1024)}, u32[]{:S(2)}) copy-start(f32[2048]{0:T(1024)} %param.20) | copy-start | bytes 24580
  0.7 5.5 %copy-start.2 = (f32[2048]{0:T(1024)S(1)}, f32[2048]{0:T(1024)}, u32[]{:S(2)}) copy-start(f32[2048]{0:T(1024)} %param.30) | copy-start | bytes 24580
  0.7 5.5 %copy-start.3 = (s32[16,2]{0,1:T(2,128)S(1)}, s32[16,2]{0,1:T(2,128)}, u32[]{:S(2)}) copy-start(s32[16,2]{0,1:T(2,128)} %param.31) | copy-start | bytes 388
  0.7 5.5 %copy-start.4 = (f32[16,2]{0,1:T(2,128)S(1)}, f32[16,2]{0,1:T(2,128)}, u32[]{:S(2)}) copy-start(f32[16,2]{0,1:T(2,128)} %param.32) | copy-start | bytes 388
  0.7 5.5 %copy-start.5 = (f32[128]{0:T(128)S(1)}, f32[128]{0:T(128)}, u32[]{:S(2)}) copy-start(f32[128]{0:T(128)} %param.28) | copy-start | bytes 1540

commit v5 on v4

--- a/solution.py
+++ b/solution.py
@@ -424,7 +424,7 @@
                 src_ref=gathered.at[slot * TILE : (slot + 1) * TILE, :],
                 dst_ref=back.at[slot * TILE : (slot + 1) * TILE, :],
                 send_sem=g_send,
-                recv_sem=g_recv,
+                recv_sem=g_recv.at[slot * 2 // plane],
                 device_id=(backward(slot), tp),
                 device_id_type=MESH,
             ).start()
@@ -435,18 +435,21 @@
         copy.wait_send()
     for swap in swaps:
         swap.wait_send()
-    landed(gathered.at[TILE : plane * TILE, :], c_send, g_recv).wait_send()
+    landed(gathered.at[TILE : plane * TILE, :], c_send, g_recv.at[0]).wait_send()
     for copies in spreads:
         for _, _, _, _, copy in copies:
             copy.wait_send()
     for _, _, copies in gives:
         for _, copy in copies:
             copy.wait_send()
-    landed(gathered.at[TILE : plane * TILE, :], g_send, g_recv).wait_send()
-
-    landed(back.at[TILE : plane * TILE, :], g_send, g_recv).wait_recv()
-    thirds = jnp.dot(combine, back[...], preferred_element_type=F32)
-    moe = thirds[:height] + thirds[height : 2 * height] + thirds[2 * height :]
+    landed(gathered.at[TILE : plane * TILE, :], g_send, g_recv.at[0]).wait_send()
+
+    middle = plane // 2 * TILE
+    moe = jnp.zeros((height, LANE), F32)
+    for half, (first, fresh, last) in enumerate(((0, TILE, middle), (middle, middle, plane * TILE))):
+        landed(back.at[fresh:last, :], g_send, g_recv.at[half]).wait_recv()
+        thirds = jnp.dot(combine[:, first:last], back[first:last, :], preferred_element_type=F32)
+        moe = moe + (thirds[:height] + thirds[height : 2 * height] + thirds[2 * height :])
     moe = jnp.concatenate([moe[q * seqs : (q + 1) * seqs] for q in range(PARTS)], axis=1)
     out_ref[...] = (resid.astype(F32) + moe).astype(BF16)
 
@@ -500,7 +503,7 @@
             dma((sum(map(len, PIECES)), lanes - 1)),
             dma((sum(map(len, PIECES)), lanes - 1)),
             dma,
-            dma,
+            dma((2,)),
         ],
         compiler_params=pltpu.CompilerParams(collective_id=0, has_side_effects=True, vmem_limit_bytes=EXCHANGE_GRANT),
     )(*small, readout, *weights, expert_gate, expert_up, expert_down)

time: 45 us -> 45 us (level)
  no operation moved by 1% of the time
where the time goes in v5:
time: 45 us; the launch traced here: 44.9 us
  Pallas kernels  43.5 us (97%)
  between operations  0.75 us (2%)
  local copies, waits for them, and re-layouts  0.63 us (1%)
    pallas_call x1, Pallas kernels, exchange(): pl.pallas_call(functools.partial(exchange_kernel, lanes, groups), name='e...  38 us
    pallas_call x1, Pallas kernels, mixer(): pl.pallas_call(functools.partial(mixer_kernel, heads), name='mixer', out_...  5.47 us

profile of v5, /device:TPU:32, one launch (start us, length us, event | category | flops | bytes accessed | tf_op | source)
XLA Modules:
  0.0 44.9 jit_solution(2214181328689896804)
XLA Ops:
  0.6 0.0 copy-start
  0.6 0.0 copy-start.1
  0.7 0.0 copy-start.2
  0.7 0.0 copy-start.3
  0.7 0.0 copy-start.4
  0.7 0.0 copy-start.5
  0.7 5.5 %mixer.1 = (f32[2048,256]{1,0:T(8,128)}, f32[16,2,128,128]{3,2,1,0:T(8,128)}) custom-call(bf16[16,2048]{1,0:T(8,128)(2,1)} %tokens.1, f32[1,2048]{1,0:T(1,128)} %bitcast.8, bf16[8,2048]{1,0:T(8,128)(2,1)} %bitcast.14, bf16[8,2048]{1,0:T(8,128)(2,1)} %bitcast.15, f32[1,8]{1,0:T(1,128)} %bitcast.16, bf16[2048,256]{1,0:T(8,128)(2,1)} %k_hbm.1, ...), custom_call_target="tpu_custom_call" | custom-call | tf_op jit(solution)/shard_map/mixer/pallas_call | solution.py:134
  6.2 0.0 copy-done
  6.2 0.0 copy-done.1
  6.2 0.0 copy-done.2
  6.2 0.0 copy-done.3
  6.2 0.0 copy-done.4
  6.2 0.0 copy-done.5
  6.2 38.0 %exchange.1 = bf16[16,512]{1,0:T(8,128)(2,1)S(1)} custom-call(bf16[16,2048]{1,0:T(8,128)(2,1)S(1)} %copy-done, f32[1,2048]{1,0:T(1,128)S(1)} %bitcast.9, f32[1,128]{1,0:T(1,128)S(1)} %bitcast.13, f32[1,2048]{1,0:T(1,128)S(1)} %bitcast.10, s32[2,16]{1,0:T(2,128)S(1)} %bitcast.11, f32[2,16]{1,0:T(2,128)S(1)} %bitcast.12, ...), custom_call_target="tpu_custom_call" | custom-call | tf_op jit(solution)/shard_map/exchange/pallas_call | solution.py:473
  44.3 0.6 %copy.21 = bf16[16,512]{1,0:T(8,128)(2,1)} copy(bf16[16,512]{1,0:T(8,128)(2,1)S(1)} %exchange.1) | data formatting | bytes 32768
Async XLA Ops:
  0.6 5.5 %copy-start = (bf16[16,2048]{1,0:T(8,128)(2,1)S(1)}, bf16[16,2048]{1,0:T(8,128)(2,1)}, u32[]{:S(2)}) copy-start(bf16[16,2048]{1,0:T(8,128)(2,1)} %tokens.1) | copy-start | bytes 196612
  0.6 5.5 %copy-start.1 = (f32[2048]{0:T(1024)S(1)}, f32[2048]{0:T(1024)}, u32[]{:S(2)}) copy-start(f32[2048]{0:T(1024)} %param.20) | copy-start | bytes 24580
  0.7 5.5 %copy-start.2 = (f32[2048]{0:T(1024)S(1)}, f32[2048]{0:T(1024)}, u32[]{:S(2)}) copy-start(f32[2048]{0:T(1024)} %param.30) | copy-start | bytes 24580
  0.7 5.5 %copy-start.3 = (s32[16,2]{0,1:T(2,128)S(1)}, s32[16,2]{0,1:T(2,128)}, u32[]{:S(2)}) copy-start(s32[16,2]{0,1:T(2,128)} %param.31) | copy-start | bytes 388
  0.7 5.5 %copy-start.4 = (f32[16,2]{0,1:T(2,128)S(1)}, f32[16,2]{0,1:T(2,128)}, u32[]{:S(2)}) copy-start(f32[16,2]{0,1:T(2,128)} %param.32) | copy-start | bytes 388
  0.7 5.5 %copy-start.5 = (f32[128]{0:T(128)S(1)}, f32[128]{0:T(128)}, u32[]{:S(2)}) copy-start(f32[128]{0:T(128)} %param.28) | copy-start | bytes 1540
